TPU v7x, 128 devices: a whole 4x4x4 slice. The times are simulated.
128 devices in a mesh: rep: 16 (over z, x), fs: 4 (over y), tp: 2 (over core).
Axes of the slice: x: 4, y: 4, z: 4, core: 2. Of those that a mesh axis runs over, the one named last changes fastest.
Arguments:
- inputs: bfloat16 [64, 768, 2048], P(('rep', 'fs'), 'tp'), may hold values from -6 to 6
- pre_gate: bfloat16 [64, 768, 2816], P(('rep', 'fs'), None, 'tp'), may hold values from -6 to 6
- pre_up: bfloat16 [64, 768, 2816], P(('rep', 'fs'), None, 'tp'), may hold values from -6 to 6
- cotangent: bfloat16 [64, 768, 2816], P(('rep', 'fs'), None, 'tp'), may hold values from -16 to 16
- w_gate: bfloat16 [2048, 2816], P('fs', 'tp'), may hold values from -0.125 to 0.125
- w_up: bfloat16 [2048, 2816], P('fs', 'tp'), may hold values from -0.125 to 0.125
- taps_gate: bfloat16 [3, 2816], replicated, may hold values from -3 to 3
- taps_up: bfloat16 [3, 2816], replicated, may hold values from -3 to 3
Outputs:
- grad_inputs: bfloat16 [64, 768, 2048], P(('rep', 'fs'), 'tp')
- grad_w_gate: float32 [2048, 2816], P('fs', 'tp')
- grad_w_up: float32 [2048, 2816], P('fs', 'tp')
- grad_taps_gate: float32 [3, 2816], replicated
- grad_taps_up: float32 [3, 2816], replicated
All inputs are finite; a program needn't handle non-finite values.
Results may differ from a plain program's by a relative error of at most 0.0059.
Values may be sent and summed in bfloat16 or wider, within the bound.
A program may use at most 192 MiB of HBM per device.

v0:
```python
import jax
import jax.numpy as jnp
from jax import lax
from jax.sharding import PartitionSpec as P


def laid_out(parts, dim):
    lengths = list(parts.shape[1:])
    lengths[dim] *= parts.shape[0]
    return jnp.moveaxis(parts, 0, dim).reshape(lengths)


def work_in_pieces(x, axis, dim, apply, out_dim):
    size, width = (lax.axis_size(axis), x.shape[dim])
    count = 2 if width % 2 == 0 else 1
    gathered, length = ([], width // count)
    for k in range(count):
        section = lax.slice_in_dim(x, k * length, (k + 1) * length, axis=dim)
        starts = jnp.arange(size) * width + k * length
        gathered.append(jax.vmap(apply)(lax.all_gather(section, axis), starts))
    return laid_out(jnp.concatenate(gathered, axis=out_dim + 1), out_dim)


def split_up(x, dim, count):
    before, after = (x.shape[:dim], x.shape[dim + 1 :])
    return jnp.moveaxis(x.reshape(*before, count, -1, *after), dim, 0)


def sum_at_owner(x, axis, dim):
    count = lax.axis_size(axis)
    parts = lax.all_to_all(split_up(x, dim, count), axis, 0, 0, tiled=True)
    return jnp.sum(parts.astype(jnp.float32), axis=0)


def side_by_side(arrays, axis, dim, along):
    widths = [a.shape[along] for a in arrays]
    both = jnp.concatenate(arrays, axis=along)
    result = lax.psum_scatter(both, axis, scatter_dimension=dim, tiled=True)
    return tuple(jnp.split(result, [sum(widths[:k]) for k in range(1, len(widths))], axis=along))


def in_one(arrays, axis):
    ravelled, at, gathered = (jnp.concatenate([a.reshape(-1) for a in arrays]), 0, [])
    subtotal = lax.psum(ravelled, axis)
    for a in arrays:
        gathered.append(subtotal[at : at + a.size].reshape(a.shape))
        at += a.size
    return tuple(gathered)


def causal_mix(signal, kernel):
    length = signal.shape[0]
    padded = jnp.pad(signal, ((2, 0), (0, 0)))
    return (
        kernel[0] * padded[0:length]
        + kernel[1] * padded[1 : length + 1]
        + kernel[2] * padded[2 : length + 2]
    )


def gated_hidden(gate_pre, up_pre, kernel_gate, kernel_up):
    return jax.nn.gelu(causal_mix(gate_pre, kernel_gate)) * causal_mix(up_pre, kernel_up)


def per_device(inputs, pre_gate, pre_up, cotangent, w_gate, w_up, taps_gate, taps_up):
    columns = pre_gate.shape[2]
    offset = lax.axis_index("tp") * columns
    kernel_gate = lax.dynamic_slice_in_dim(taps_gate, offset, columns, 1).astype(jnp.float32)
    kernel_up = lax.dynamic_slice_in_dim(taps_up, offset, columns, 1).astype(jnp.float32)
    _, pullback = jax.vjp(
        gated_hidden,
        pre_gate[0].astype(jnp.float32),
        pre_up[0].astype(jnp.float32),
        kernel_gate,
        kernel_up,
    )
    back_gate, back_up, tap_gate, tap_up = pullback(cotangent[0].astype(jnp.float32))
    stacked = jnp.stack([back_gate, back_up], axis=1).astype(jnp.bfloat16)
    weights = jnp.stack([w_gate, w_up])

    def project(weight_block, row_start):
        return jnp.einsum("lkf,knf->ln", stacked, weight_block, preferred_element_type=jnp.float32)

    partial_value = work_in_pieces(weights, "fs", 1, project, 1)
    grad_inputs = sum_at_owner(partial_value.astype(jnp.bfloat16), "tp", 0).astype(jnp.bfloat16)[
        None
    ]
    rep_count = lax.axis_size("rep")
    shard_count = lax.axis_size("fs")
    features = inputs.shape[2]
    layout = (shard_count, features // shard_count)
    pattern = "nfd,nk->fdk"
    token_block = lax.all_gather(inputs, "tp", axis=1, tiled=True)
    row_count = token_block.shape[1]
    spread = token_block[0].reshape((row_count,) + layout)
    gate_total = jnp.einsum(pattern, spread, stacked[:, 0], preferred_element_type=jnp.float32)
    up_total = jnp.einsum(pattern, spread, stacked[:, 1], preferred_element_type=jnp.float32)
    factor = float(pre_gate.shape[1] * rep_count * shard_count) ** (-0.5)
    pieces = side_by_side((gate_total, up_total), "fs", 0, 1)
    whole = lax.psum((pieces[0], pieces[1]), "rep")
    grad_w_gate = whole[0].reshape(features // shard_count, columns) * factor
    grad_w_up = whole[1].reshape(features // shard_count, columns) * factor
    blank = jnp.zeros(taps_gate.shape, jnp.float32)
    full_gate = lax.dynamic_update_slice_in_dim(blank, tap_gate, offset, 1)
    full_up = lax.dynamic_update_slice_in_dim(blank, tap_up, offset, 1)
    summed_gate, summed_up = in_one((full_gate, full_up), ("rep", "fs", "tp"))
    return (grad_inputs, grad_w_gate, grad_w_up, summed_gate * factor, summed_up * factor)


def solution(mesh):
    placed = (
        P(("rep", "fs"), "tp", None),
        P(("rep", "fs"), None, "tp"),
        P(("rep", "fs"), None, "tp"),
        P(("rep", "fs"), None, "tp"),
        P("fs", "tp"),
        P("fs", "tp"),
        P(),
        P(),
    )
    return jax.shard_map(
        per_device,
        mesh=mesh,
        in_specs=placed,
        out_specs=(P(("rep", "fs"), "tp", None), P("fs", "tp"), P("fs", "tp"), P(), P()),
        check_vma=False,
    )
```

profile of v0, /device:TPU:1, one launch (start us, length us, event | category | flops | bytes accessed | tf_op | source)
XLA Modules:
  0.0 535.5 jit_solution(3696512987416850347)
XLA Ops:
  8.0 0.0 all-gather.6.cloned.1.call-start
  8.0 0.7 all-gather.6.cloned.1.call-update
  8.7 0.0 reduce-scatter.2.cloned.1.call-start
  8.8 0.7 dynamic-slice_convert_fusion
  9.6 0.1 slice_reduce_fusion.5
  9.6 0.0 copy-start
  9.6 0.0 copy-start.2
  9.6 3.0 bitcast_convert_fusion.2
  12.6 0.0 copy-done
  12.6 0.6 copy-done.2
  13.2 0.0 copy-start.1
  13.2 7.1 %multiply_reduce_fusion.4 = (f32[1408]{0:T(1024)S(1)}, f32[1408]{0:T(1024)S(1)}, f32[1408]{0:T(1024)S(1)}, f32[768,1408]{1,0:T(8,128)S(1)}, f32[768,1408]{1,0:T(8,128)S(1)}) fusion(f32[768,1408]{1,0:T(8,128)S(1)} %get-tuple-element.41, bf16[1,768,1408]{2,1,0:T(8,128)(2,1)S(1)} %copy-done, f32[768,1408]{1,0:T(8,128)S(1)} %get-tuple-element.42, ...), kind=kLoop, calls=%fused_computation.24 | loop fusion | flops 41086848 | bytes 21677568 | tf_op jit(solution)/shard_map/transpose(jvp())/reduce_sum | solution.py:56
  20.3 0.0 copy-done.1
  20.3 4.6 multiply_reduce_fusion.1
  25.0 2.8 broadcast_multiply_fusion.2
  27.8 4.8 fusion.6
  32.6 0.8 broadcast_multiply_fusion.5
  33.4 2.3 fusion.7
  35.8 0.0 all-gather.6.cloned.1.call-done
  35.8 3.4 copy.16
  39.2 0.0 copy-start.5
  39.2 7.3 %convolution_bitcast_fusion = f32[4,512,1408]{2,1,0:T(8,128)S(1)} fusion(bf16[768,4,512]{0,2,1:T(8,128)(2,1)S(1)} %bitcast.73, bf16[768,1408]{1,0:T(8,128)(2,1)} %fusion.6), kind=kOutput, calls=%fused_computation.1 | convolution fusion | flops 4429185024 | bytes 16842752 | tf_op jit(solution)/shard_map/nfd,nk->fdk/dot_general | solution.py:97
  46.5 0.0 copy-done.5
  46.5 5.5 %convolution_bitcast_fusion.1 = f32[4,512,1408]{2,1,0:T(8,128)S(1)} fusion(bf16[768,4,512]{0,2,1:T(8,128)(2,1)S(1)} %bitcast.74, bf16[768,1408]{1,0:T(8,128)(2,1)S(1)} %copy-done.5), kind=kOutput, calls=%fused_computation.2 | convolution fusion | flops 4429185024 | bytes 16842752 | tf_op jit(solution)/shard_map/nfd,nk->fdk/dot_general | solution.py:96
  52.0 9.1 %pad_maximum_fusion = f32[4,1024,1408]{2,1,0:T(8,128)} fusion(f32[4,512,1408]{2,1,0:T(8,128)S(1)} %convolution_bitcast_fusion, f32[4,512,1408]{2,1,0:T(8,128)S(1)} %convolution_bitcast_fusion.1), kind=kLoop, calls=%fused_computation | loop fusion | flops 5767168 | bytes 46137344 | tf_op jit(solution)/shard_map/concatenate | solution.py:37
  61.1 0.0 copy-start.7
  61.1 0.0 reduce-scatter.2.cloned.1.call-update
  61.2 0.0 all-reduce.18.cloned.1.call-start
  61.4 0.6 pad_maximum_fusion.2
  62.1 0.0 all-reduce.18.cloned.1.call-update
  62.1 0.0 all-gather.10.cloned.1.call-start
  62.2 0.4 copy-done.7
  62.5 0.4 copy-done.8
  62.9 1.8 fusion.14
  64.7 0.0 all-gather.10.cloned.1.call-update
  64.8 0.0 all-gather.8.cloned.1.call-start
  64.8 0.5 all-gather.8.cloned.1.call-update
  65.3 0.3 all-reduce.20.cloned.1.call-start
  65.6 198.4 %reduce-scatter.2.cloned.1.call-done = f32[1,1024,1408]{2,1,0:T(8,128)} async-done(((f32[4,1024,1408]{2,1,0:T(8,128)}), f32[1,1024,1408]{2,1,0:T(8,128)}) %reduce-scatter.2.cloned.1.call-update) | async-done | bytes 5767184 | tf_op jit(solution)/shard_map/reduce_scatter | solution.py:38
  264.0 5.6 %fusion.18 = (f32[1,512,1408]{2,1,0:T(8,128)}, f32[1,512,1408]{2,1,0:T(8,128)}) fusion(f32[1,1024,1408]{2,1,0:T(8,128)} %reduce-scatter.2.cloned.1.call-done), kind=kLoop, calls=%fused_computation.69 | loop fusion | bytes 11534336 | tf_op jit(solution)/shard_map/split | solution.py:39
  269.6 0.0 copy-start.4
  269.6 0.0 all-reduce.20.cloned.1.call-update
  269.6 134.9 %all-reduce.18.cloned.1.call-done = f32[16896]{0:T(1024)} async-done(((f32[16896]{0:T(1024)}), f32[16896]{0:T(1024)}) %all-reduce.18.cloned.1.call-update) | async-done | bytes 67600 | tf_op jit(solution)/shard_map/psum | solution.py:44
  404.5 0.9 slice_multiply_fusion
  405.4 0.6 mul.244
  406.0 0.6 mul.246
  406.6 0.0 all-gather.10.cloned.1.call-done
  406.6 0.0 copy-done.4
  406.6 9.1 %fusion.13 = bf16[4,768,256]{1,2,0:T(8,128)(2,1)} fusion(bf16[4,2,256,1408]{3,2,1,0:T(8,128)(2,1)} %bitcast.81, bf16[768,1,1408]{2,0,1:T(8,128)(2,1)S(1)} %bitcast.75, bf16[768,1,1408]{2,0,1:T(8,128)(2,1)} %bitcast.77), kind=kOutput, calls=%fused_computation.51 | convolution fusion | flops 4438622208 | bytes 11665408 | tf_op jit(solution)/shard_map/vmap(lkf,knf->ln)/dot_general | solution.py:82
  415.7 0.0 all-gather.8.cloned.1.call-done
  415.7 0.0 copy-start.6
  415.7 8.1 %fusion.12 = bf16[4,768,256]{1,2,0:T(8,128)(2,1)S(1)} fusion(bf16[4,2,256,1408]{3,2,1,0:T(8,128)(2,1)} %bitcast.82, bf16[768,1,1408]{2,0,1:T(8,128)(2,1)S(1)} %bitcast.76, bf16[768,1,1408]{2,0,1:T(8,128)(2,1)} %bitcast.78), kind=kOutput, calls=%fused_computation.50 | convolution fusion | flops 4438622208 | bytes 11665408 | tf_op jit(solution)/shard_map/vmap(lkf,knf->ln)/dot_general | solution.py:82
  423.8 0.0 copy-done.6
  423.8 0.2 maximum_bitcast_fusion.1
  424.0 2.4 convert_element_type.47
  426.5 2.3 copy.14
  428.8 5.9 %all_to_all.5 = bf16[2,384,2048]{1,2,0:T(8,128)(2,1)S(1)} all-to-all(bf16[2,384,2048]{1,2,0:T(8,128)(2,1)S(1)} %copy.14), channel_id=1, replica_groups=mesh['rep'=16,'fs'=4,'tp'=2] {'tp'}, dimensions={0} | all-to-all | bytes 6291456 | tf_op jit(solution)/shard_map/all_to_all | solution.py:31
  434.7 2.2 reduce_sum.65
  436.8 2.6 copy.17
  439.4 83.4 %all-reduce.20.cloned.1.call-done = (f32[1,512,1408]{2,1,0:T(8,128)}, f32[1,512,1408]{2,1,0:T(8,128)}) async-done(((f32[1,512,1408]{2,1,0:T(8,128)}, f32[1,512,1408]{2,1,0:T(8,128)}), (f32[1,512,1408]{2,1,0:T(8,128)}, f32[1,512,1408]{2,1,0:T(8,128)})) %all-reduce.20.cloned.1.call-update) | async-done | bytes 5767184 | tf_op jit(solution)/shard_map/psum | solution.py:100
  522.8 0.0 copy-start.3
  522.8 3.8 multiply_bitcast_fusion.1
  526.6 0.0 copy-done.3
  526.6 1.8 multiply_bitcast_fusion
  (14 shorter events, 0.2 us)
Async XLA Ops:
  8.0 27.8 %all-gather.6.cloned.1.call-start = ((), (), s32[]{:S(2)}) async-start(), calls=%async_computation.2 | async-start | bytes 4718592 | tf_op jit(solution)/shard_map/all_gather | solution.py:93
  8.7 255.2 %reduce-scatter.2.cloned.1.call-start = ((), (), s32[]{:S(2)}) async-start(), calls=%async_computation.3 | async-start | bytes 28835840 | tf_op jit(solution)/shard_map/reduce_scatter | solution.py:38
  9.6 3.0 copy-start
  9.6 3.6 copy-start.2
  13.2 7.1 %copy-start.1 = (bf16[1,768,1408]{2,1,0:T(8,128)(2,1)S(1)}, bf16[1,768,1408]{2,1,0:T(8,128)(2,1)}, u32[]{:S(2)}) copy-start(bf16[1,768,1408]{2,1,0:T(8,128)(2,1)} %param.10) | copy-start | bytes 6488068
  39.2 7.3 %copy-start.5 = (bf16[768,1408]{1,0:T(8,128)(2,1)S(1)}, bf16[768,1408]{1,0:T(8,128)(2,1)}, u32[]{:S(2)}) copy-start(bf16[768,1408]{1,0:T(8,128)(2,1)} %fusion.7) | copy-start | bytes 6488068
  61.1 1.4 copy-start.7
  61.1 1.8 copy-start.8
  61.2 343.4 %all-reduce.18.cloned.1.call-start = ((), (), s32[]{:S(2)}) async-start(), calls=%async_computation.4 | async-start | bytes 139264 | tf_op jit(solution)/shard_map/psum | solution.py:44
  62.1 344.5 %all-gather.10.cloned.1.call-start = ((), (), s32[]{:S(2)}) async-start(), calls=%async_computation.6 | async-start | bytes 7208960 | tf_op jit(solution)/shard_map/all_gather | solution.py:20
  64.8 351.0 %all-gather.8.cloned.1.call-start = ((), (), s32[]{:S(2)}) async-start(), calls=%async_computation.5 | async-start | bytes 7208960 | tf_op jit(solution)/shard_map/all_gather | solution.py:20
  65.3 457.5 %all-reduce.20.cloned.1.call-start = ((), (), s32[]{:S(2)}) async-start(), calls=%async_computation.7 | async-start | bytes 11534336 | tf_op jit(solution)/shard_map/psum | solution.py:100
  269.6 137.1 %copy-start.4 = (bf16[768,1408]{1,0:T(8,128)(2,1)S(1)}, bf16[768,1408]{1,0:T(8,128)(2,1)}, u32[]{:S(2)}) copy-start(bf16[768,1408]{1,0:T(8,128)(2,1)} %fusion.6) | copy-start | bytes 6488068
  415.7 8.1 %copy-start.6 = (bf16[4,768,256]{1,2,0:T(8,128)(2,1)S(1)}, bf16[4,768,256]{1,2,0:T(8,128)(2,1)}, u32[]{:S(2)}) copy-start(bf16[4,768,256]{1,2,0:T(8,128)(2,1)} %fusion.13) | copy-start | bytes 4718596
  522.8 3.8 copy-start.3
Sparse Core Ops, SparseCore 0:
  10.5 18.4 all-gather.5
  61.3 202.6 reduce-scatter.1
  266.2 60.8 all-gather.9
  328.6 61.9 all-gather.7
Sparse Core Ops, SparseCore 1:
  66.4 338.1 all-reduce.17
  408.4 114.3 all-reduce.19
where the time goes:
time: 536 us
  waiting for transfers between devices  418 us (78%)
  other arithmetic  46.8 us (9%)
  matrix products  29.9 us (6%)
  local copies, waits for them, and re-layouts  19.1 us (4%)
  between operations  15.4 us (3%)
  blocking collectives  5.9 us (1%)
    reduce_scatter x1, waiting for transfers between devices, side_by_side(): result = lax.psum_scatter(both, axis, scatter_dimension=dim, tiled=True)  198 us
    psum x1, waiting for transfers between devices, in_one(): subtotal = lax.psum(ravelled, axis)  135 us
    psum x1, waiting for transfers between devices, per_device(): whole = lax.psum((pieces[0], pieces[1]), 'rep')  83.4 us
    dot_general x2, matrix products, project(): jnp.einsum('lkf,knf->ln', stacked, weight_block, preferred_element_type=j...  17.1 us
    reduce_sum x2, other arithmetic, causal_mix(): kernel[1] * padded[1:length + 1]  11.8 us
  transfers between devices with their start and end apart: 6, of which 3 were waited for; matrix products, arithmetic and copies ran while one was open for 12% of the time, Pallas kernels for 0%

commit v1 on v0

v1 whole, which is shorter than its diff:
```python
import functools

import jax
import jax.numpy as jnp
from jax import lax
from jax.experimental import pallas as pl
from jax.experimental.pallas import tpu as pltpu
from jax.sharding import PartitionSpec as P

MESH = pl.DeviceIdType.MESH
LEN = 768
COLS = 1408
WIDTH = 2048
TOKENS = 49152
SPLITS = ((0, 640), (640, 768))
CHUNK = 64
PAD = 16
HALF = LEN // 2
ROOT = 0.7978845608028654
CUBIC = 0.044715
bf16, f32 = jnp.bfloat16, jnp.float32


def wrap(value, n=4):
    return lax.rem(value + 2 * n, n)


def mult(value, n):
    return pl.multiple_of(value, n)


def kernel(
    x_hbm, pg_hbm, pu_hbm, ct_hbm, wg_hbm, wu_hbm, tg_ref, tu_ref,
    gi_out, ag_out, tog_ref, tou_ref,
    pg, pu, ct, xs, xt, wall, buf0, buf1, own, acc1, two0, two1, acc2,
    out3_0, out3_1, in3_0, in3_1, ag, taps, tfin, gsend, gown, grecv,
    loc, xsem, w1s, w1r, w2s, w2r, p1s, p1r, p2s, p2r, p3s, p3r,
    a1s, a1r, a2s, a2r, a3s, a3r, tss, tsr, gss, gsr,
):
    rep, y, c = lax.axis_index("rep"), lax.axis_index("fs"), lax.axis_index("tp")
    z, x = rep // 4, lax.rem(rep, 4)
    first, second = (x, z), (z, x)
    bufs, twos = (buf0, buf1), (two0, two1)
    outs3, ins3 = (out3_0, out3_1), (in3_0, in3_1)

    def dev(dx=0, dz=0, dy=0, dc=0):
        return (wrap(z + dz) * 4 + wrap(x + dx), wrap(y + dy), wrap(c + dc, 2))

    def first_dev(p, d):
        return dev(dx=d) if p == 0 else dev(dz=d)

    def second_dev(p, d):
        return dev(dz=d) if p == 0 else dev(dx=d)

    def remote(src, dst, send, recv, where):
        return pltpu.make_async_remote_copy(
            src_ref=src, dst_ref=dst, send_sem=send, recv_sem=recv, device_id=where, device_id_type=MESH
        )

    started = []

    def send(src, dst, send_sem, recv_sem, where):
        copy = remote(src, dst, send_sem, recv_sem, where)
        copy.start()
        started.append(copy)
        return copy

    local = []

    def load(src, dst):
        copy = pltpu.make_async_copy(src, dst, loc.at[len(local)])
        copy.start()
        local.append(copy)
        return copy

    pre = []
    for at, width in SPLITS:
        cols = pl.ds(at, width)
        pre.append(
            [load(h.at[0, :, cols], v.at[pl.ds(PAD, LEN), cols]) for h, v in ((pg_hbm, pg), (pu_hbm, pu), (ct_hbm, ct))]
        )
    mine = pl.ds(mult(c * HALF, HALF), HALF)
    x_local = load(x_hbm.at[0], xs.at[mine])
    w_local = [load(h, wall.at[g, y]) for g, h in enumerate((wg_hbm, wu_hbm))]
    pg[0:PAD, :] = jnp.zeros((PAD, COLS), bf16)
    pu[0:PAD, :] = jnp.zeros((PAD, COLS), bf16)

    peers = [dev(dx=d) for d in (1, 2, 3)] + [dev(dz=d) for d in (1, 2, 3)]
    peers += [dev(dy=d) for d in (1, 2, 3)] + [dev(dc=1)]
    barrier = pltpu.get_barrier_semaphore()
    for peer in peers:
        pl.semaphore_signal(barrier, inc=1, device_id=peer, device_id_type=MESH)
    pl.semaphore_wait(barrier, len(peers))

    x_send = send(x_hbm.at[0], xs.at[mine], xsem.at[0], xsem.at[1], dev(dc=1))
    hbm_w = (wg_hbm, wu_hbm)

    def w_rows(half):
        return pl.ds(half * 256, 256)

    for order in range(2):
        for g in range(2):
            for way in range(2):
                half = order if way == 0 else 1 - order
                index = way * 4 + order * 2 + g
                send(
                    hbm_w[g].at[w_rows(half)], wall.at[g, y, w_rows(half)], w1s.at[index], w1r.at[index],
                    dev(dy=1 if way == 0 else -1),
                )

    def w_arrived(way, order, g):
        half = order if way == 0 else 1 - order
        index = way * 4 + order * 2 + g
        place = wall.at[g, wrap(y - 1 if way == 0 else y + 1), w_rows(half)]
        remote(place, place, w1s.at[index], w1r.at[index], dev(dy=1)).wait_recv()

    def w_forward(g):
        for way in range(2):
            w_arrived(way, 0, g)
            place = wall.at[g, wrap(y - 1 if way == 0 else y + 1), w_rows(way)]
            send(place, place, w2s.at[way * 2 + g], w2r.at[way * 2 + g], dev(dy=1 if way == 0 else -1))

    def w_far_arrived(way, g):
        place = wall.at[g, wrap(y + 2), w_rows(way)]
        remote(place, place, w2s.at[way * 2 + g], w2r.at[way * 2 + g], dev(dy=1)).wait_recv()

    def elementwise(k):
        at, width = SPLITS[k]

        def column(b, _):
            col = mult(at + b * 128, 128)
            cols = pl.ds(col, 128)
            shared = pl.ds(mult(c * COLS + col, 128), 128)
            kg = tg_ref[:, shared].astype(f32)
            ku = tu_ref[:, shared].astype(f32)
            kg = [kg[j : j + 1] for j in range(3)]
            ku = [ku[j : j + 1] for j in range(3)]

            def rows(i, carry):
                next_g, next_u, sums = carry
                r = mult(LEN - CHUNK - i * CHUNK, CHUNK)
                span, here = pl.ds(r, CHUNK + PAD), pl.ds(r + PAD, CHUNK)
                eg = pg[span, cols].astype(f32)[8:]
                eu = pu[span, cols].astype(f32)[8:]
                co = ct[here, cols].astype(f32)
                sg = [pltpu.roll(eg, 2, 0)[8:], pltpu.roll(eg, 1, 0)[8:], eg[8:]]
                su = [pltpu.roll(eu, 2, 0)[8:], pltpu.roll(eu, 1, 0)[8:], eu[8:]]
                v = kg[0] * sg[0] + kg[1] * sg[1] + kg[2] * sg[2]
                m = ku[0] * su[0] + ku[1] * su[1] + ku[2] * su[2]
                v2 = v * v
                t = jnp.tanh(v * (ROOT + (ROOT * CUBIC) * v2))
                h = 0.5 + 0.5 * t
                slope = h * (1.0 + v * (1.0 - t) * (ROOT + (3.0 * ROOT * CUBIC) * v2))
                bg = co * m * slope
                bu = co * (v * h)
                new = tuple(
                    s + (back * moved).reshape(CHUNK // 8, 8, 128).sum(0)
                    for s, (back, moved) in zip(sums, [(bg, q) for q in sg] + [(bu, q) for q in su])
                )
                for ref, back, after, taps_of in ((pg, bg, next_g, kg), (pu, bu, next_u, ku)):
                    whole = jnp.concatenate([back, after], axis=0)
                    one = pltpu.roll(whole, CHUNK + 7, 0)[:CHUNK]
                    two = pltpu.roll(whole, CHUNK + 6, 0)[:CHUNK]
                    ref[here, cols] = (taps_of[2] * back + taps_of[1] * one + taps_of[0] * two).astype(bf16)
                return bg[:8], bu[:8], new

            zero = jnp.zeros((8, 128), f32)
            _, _, sums = lax.fori_loop(0, LEN // CHUNK, rows, (zero, zero, (zero,) * 6))
            rows8 = [jnp.sum(s, axis=0, keepdims=True) for s in sums]
            taps[0, x, :, cols] = jnp.concatenate(rows8 + [jnp.zeros((2, 128), f32)], axis=0)
            return 0

        lax.fori_loop(0, width // 128, column, 0)

    grads = (pg, pu)

    def own_rows(p, s):
        parts = []
        for yb in range(4):
            chunk = wrap(first[p] - 1 - s) if yb < 2 else wrap(first[p] + 1 + s)
            parts.append(xt[pl.ds(mult(yb * 512 + chunk * 128, 128), 128), :])
        return jnp.concatenate(parts, axis=0)

    def product(p, k, s):
        at, width = SPLITS[k]
        right = grads[p][PAD : PAD + LEN, at : at + width]
        return jnp.dot(own_rows(p, s), right, preferred_element_type=f32).reshape(4, 128, width)

    def p1_index(k, p, way, s):
        return ((k * 2 + p) * 2 + way) * 3 + s

    def p1_copy(k, p, way, s):
        pair = pl.ds(way * 2, 2)
        index = p1_index(k, p, way, s)
        return (
            bufs[k].at[p, s, pair], bufs[k].at[p, s + 1, pair], p1s.at[index], p1r.at[index],
            first_dev(p, 1 if way == 0 else -1),
        )

    def step0(k):
        for p in range(2):
            bufs[k][p, 0] = product(p, k, 0).astype(bf16)
            for way in range(2):
                send(*p1_copy(k, p, way, 0))

    def step1(k, s):
        at, width = SPLITS[k]
        for p in range(2):
            own[p, :, :, 0:width] = product(p, k, s)
        for p in range(2):
            for way in range(2):
                remote(*p1_copy(k, p, way, s - 1)).wait_recv()

            def add(yb, _):
                total = bufs[k][p, s, yb].astype(f32) + own[p, yb, :, 0:width]
                if s < 3:
                    bufs[k][p, s, yb] = total.astype(bf16)
                else:
                    acc1[p, yb, :, at : at + width] = total
                return 0

            lax.fori_loop(0, 4, add, 0)
            if s < 3:
                for way in range(2):
                    send(*p1_copy(k, p, way, s))

    def p2_copy(k, p, way, s):
        pair = pl.ds(way * 2, 2)
        index = p1_index(k, p, way, s)
        return (
            twos[k].at[p, s, pair], twos[k].at[p, s + 1, pair], p2s.at[index], p2r.at[index],
            second_dev(p, 1 if way == 0 else -1),
        )

    def step2(k, s):
        at, width = SPLITS[k]
        for p in range(2):
            if s > 0:
                for way in range(2):
                    remote(*p2_copy(k, p, way, s - 1)).wait_recv()

            def add(yb, _):
                move = (1 - 2 * (yb // 2)) * (1 + s)
                chunk = wrap(second[p] - move)
                total = acc1[p, yb, pl.ds(mult(chunk * 32, 32), 32), at : at + width]
                if s > 0:
                    total = total + twos[k][p, s, yb].astype(f32)
                if s < 3:
                    twos[k][p, s, yb] = total.astype(bf16)
                else:
                    acc2[p, yb, :, at : at + width] = total
                return 0

            lax.fori_loop(0, 4, add, 0)
            if s < 3:
                for way in range(2):
                    send(*p2_copy(k, p, way, s))

    def p3_copy(k, p, d):
        index = (k * 2 + p) * 3 + d - 1
        return outs3[k].at[p, d - 1], ins3[k].at[p, d - 1], p3s.at[index], p3r.at[index], dev(dy=d)

    def p3_send(k):
        at, width = SPLITS[k]
        for p in range(2):
            for d in (1, 3, 2):
                outs3[k][p, d - 1] = acc2[p, wrap(y + d), :, at : at + width].astype(bf16)
                send(*p3_copy(k, p, d))

    def block(p, d_first, d_second, skip=0, rows=32):
        start = wrap(first[p] + d_first) * 128 + wrap(second[p] + d_second) * 32 + skip
        return ag.at[p, pl.ds(mult(start, 16), rows)]

    def p3_finish(k, p):
        at, width = SPLITS[k]
        total = acc2[p, y, :, at : at + width]
        for d in (1, 3, 2):
            remote(*p3_copy(k, p, d)).wait_recv()
            total = total + ins3[k][p, d - 1].astype(f32)
        start = mult(first[p] * 128 + second[p] * 32, 32)
        ag[p, pl.ds(start, 32), at : at + width] = total.astype(bf16)

    def a1_start(p):
        for d in (1, 3, 2):
            index = p * 3 + d - 1
            place = block(p, 0, 0)
            send(place, place, a1s.at[index], a1r.at[index], second_dev(p, d))

    def a1_wait(p, d):
        index = p * 3 + d - 1
        place = block(p, 0, -d)
        remote(place, place, a1s.at[index], a1r.at[index], second_dev(p, d)).wait_recv()

    def a2_start(p, d):
        for way in range(2):
            index = (p * 2 + way) * 4 + d
            place = block(p, 0, -d)
            send(place, place, a2s.at[index], a2r.at[index], first_dev(p, 1 if way == 0 else -1))

    def a2_pass_on(p, d):
        for way in range(2):
            index = (p * 2 + way) * 4 + d
            from_ = -1 if way == 0 else 1
            place = block(p, from_, -d)
            remote(place, place, a2s.at[index], a2r.at[index], first_dev(p, 1)).wait_recv()
            part = block(p, from_, -d, 16 * way, 16)
            send(part, part, a3s.at[index], a3r.at[index], first_dev(p, -from_))

    def a3_wait(p, d):
        for way in range(2):
            index = (p * 2 + way) * 4 + d
            place = block(p, 2, -d, 16 * way, 16)
            remote(place, place, a3s.at[index], a3r.at[index], first_dev(p, 1)).wait_recv()

    coords = (x, z, y)

    def tap_dev(stage, d):
        return dev(dx=d) if stage == 0 else dev(dz=d) if stage == 1 else dev(dy=d)

    def tap_send(stage):
        place = taps.at[stage, coords[stage]]
        for d in (1, 2, 3):
            index = stage * 3 + d - 1
            send(place, place, tss.at[index], tsr.at[index], tap_dev(stage, d))

    def tap_sum(stage):
        for d in (1, 2, 3):
            index = stage * 3 + d - 1
            place = taps.at[stage, wrap(coords[stage] - d)]
            remote(place, place, tss.at[index], tsr.at[index], tap_dev(stage, d)).wait_recv()
        total = taps[stage, 0] + taps[stage, 1] + taps[stage, 2] + taps[stage, 3]
        if stage < 2:
            taps[stage + 1, coords[stage + 1]] = total
            tap_send(stage + 1)
        else:
            tfin[c] = total * (float(TOKENS) ** -0.5)
            send(tfin.at[c], tfin.at[c], tss.at[9], tsr.at[9], dev(dc=1))

    def tap_end():
        other = tfin.at[wrap(c + 1, 2)]
        remote(other, other, tss.at[9], tsr.at[9], dev(dc=1)).wait_recv()
        for side in range(2):
            cols = slice(side * COLS, side * COLS + COLS)
            tog_ref[:, cols] = tfin[side, 0:3]
            tou_ref[:, cols] = tfin[side, 3:6]

    def project(unit, d, half):
        shard = wrap(y + d)

        def side(which, _):
            to_partner = 1 - which
            row = mult(PAD + wrap(c + to_partner, 2) * HALF, 16)
            value = lax.dot_general(
                pg[pl.ds(row, HALF), :], wall[0, shard, half * 256 : half * 256 + 256, :],
                (((1,), (1,)), ((), ())), preferred_element_type=f32,
            )
            value = value + lax.dot_general(
                pu[pl.ds(row, HALF), :], wall[1, shard, half * 256 : half * 256 + 256, :],
                (((1,), (1,)), ((), ())), preferred_element_type=f32,
            )
            gsend[which, unit] = value.astype(bf16)
            return 0

        lax.fori_loop(0, 2, side, 0)
        send(gsend.at[0, unit], grecv.at[unit], gss.at[unit], gsr.at[unit], dev(dc=1))

    out_copies = []

    def combine(unit, d, half):
        remote(gsend.at[0, unit], grecv.at[unit], gss.at[unit], gsr.at[unit], dev(dc=1)).wait_recv()
        gown[unit] = (gsend[1, unit].astype(f32) + grecv[unit].astype(f32)).astype(bf16)
        col = mult(wrap(y + d) * 512 + half * 256, 256)
        out_copies.append(load(gown.at[unit], gi_out.at[:, pl.ds(col, 256)]))

    for copy in pre[0]:
        copy.wait()
    elementwise(0)
    x_local.wait()
    other = xs.at[pl.ds(mult(wrap(c + 1, 2) * HALF, HALF), HALF)]
    remote(other, other, xsem.at[0], xsem.at[1], dev(dc=1)).wait_recv()

    def turn(b, _):
        at = mult(b * 128, 128)
        xt[pl.ds(at, 128), :] = xs[:, pl.ds(at, 128)].T
        return 0

    lax.fori_loop(0, WIDTH // 128, turn, 0)
    step0(0)
    for copy in pre[1]:
        copy.wait()
    elementwise(1)
    step0(1)
    tap_send(0)
    step1(0, 1)
    step1(1, 1)
    tap_sum(0)
    for copy in w_local:
        copy.wait()
    project(0, 0, 0)
    step1(0, 2)
    project(1, 0, 1)
    step1(1, 2)
    tap_sum(1)
    w_forward(0)
    combine(0, 0, 0)
    combine(1, 0, 1)
    step1(0, 3)
    step2(0, 0)
    w_arrived(0, 0, 1)
    w_arrived(1, 0, 1)
    project(2, -1, 0)
    step1(1, 3)
    step2(1, 0)
    tap_sum(2)
    project(3, 1, 1)
    step2(0, 1)
    step2(1, 1)
    combine(2, -1, 0)
    combine(3, 1, 1)
    step2(0, 2)
    step2(1, 2)
    for g in range(2):
        w_arrived(0, 1, g)
        w_arrived(1, 1, g)
    project(4, -1, 1)
    step2(0, 3)
    p3_send(0)
    step2(1, 3)
    p3_send(1)
    for way in range(2):
        place = wall.at[1, wrap(y - 1 if way == 0 else y + 1), w_rows(way)]
        send(place, place, w2s.at[way * 2 + 1], w2r.at[way * 2 + 1], dev(dy=1 if way == 0 else -1))
    project(5, 1, 0)
    for p in range(2):
        p3_finish(0, p)
    for p in range(2):
        p3_finish(1, p)
        a1_start(p)
        a2_start(p, 0)
    for d in (1, 3, 2):
        for p in range(2):
            a1_wait(p, d)
            a2_start(p, d)
    combine(4, -1, 1)
    combine(5, 1, 0)
    tap_end()
    for d in (0, 1, 3, 2):
        for p in range(2):
            a2_pass_on(p, d)
    for way in range(2):
        for g in range(2):
            w_far_arrived(way, g)
    project(6, 2, 0)
    project(7, 2, 1)
    for d in (0, 1, 3, 2):
        for p in range(2):
            a3_wait(p, d)
    for p in range(2):
        out_copies.append(load(ag.at[p], ag_out.at[p]))
    combine(6, 2, 0)
    combine(7, 2, 1)
    for copy in started:
        copy.wait_send()
    for copy in out_copies:
        copy.wait()


def per_device(inputs, pre_gate, pre_up, cotangent, w_gate, w_up, taps_gate, taps_up):
    any_ = pl.BlockSpec(memory_space=pl.ANY)
    vmem = pl.BlockSpec(memory_space=pltpu.VMEM)
    dma = pltpu.SemaphoreType.DMA
    widths = [width for _, width in SPLITS]
    scratch = (
        [pltpu.VMEM((PAD + LEN, COLS), bf16)] * 3
        + [pltpu.VMEM((LEN, WIDTH), bf16), pltpu.VMEM((WIDTH, LEN), bf16), pltpu.VMEM((2, 4, 512, COLS), bf16)]
        + [pltpu.VMEM((2, 4, 4, 128, width), bf16) for width in widths]
        + [pltpu.VMEM((2, 4, 128, max(widths)), f32), pltpu.VMEM((2, 4, 128, COLS), f32)]
        + [pltpu.VMEM((2, 4, 4, 32, width), bf16) for width in widths]
        + [pltpu.VMEM((2, 4, 32, COLS), f32)]
        + [pltpu.VMEM((2, 3, 32, width), bf16) for width in widths] * 2
        + [pltpu.VMEM((2, 512, COLS), bf16), pltpu.VMEM((3, 4, 8, COLS), f32), pltpu.VMEM((2, 8, COLS), f32)]
        + [pltpu.VMEM((2, 8, HALF, 256), bf16), pltpu.VMEM((8, HALF, 256), bf16), pltpu.VMEM((8, HALF, 256), bf16)]
        + [dma((32,)), dma((2,)), dma((8,)), dma((8,)), dma((4,)), dma((4,))]
        + [dma((24,))] * 4
        + [dma((12,))] * 2
        + [dma((6,))] * 2
        + [dma((16,))] * 4
        + [dma((10,))] * 2
        + [dma((8,))] * 2
    )
    grad_inputs, sums, tap_gate, tap_up = pl.pallas_call(
        kernel,
        out_shape=(
            jax.ShapeDtypeStruct((HALF, WIDTH), bf16),
            jax.ShapeDtypeStruct((2, 512, COLS), bf16),
            jax.ShapeDtypeStruct((3, 2 * COLS), f32),
            jax.ShapeDtypeStruct((3, 2 * COLS), f32),
        ),
        in_specs=[any_] * 6 + [vmem] * 2,
        out_specs=(any_, any_, vmem, vmem),
        scratch_shapes=scratch,
        compiler_params=pltpu.CompilerParams(
            collective_id=0, has_side_effects=True, vmem_limit_bytes=67043328
        ),
    )(inputs, pre_gate, pre_up, cotangent, w_gate, w_up, taps_gate, taps_up)
    factor = float(TOKENS) ** -0.5
    return (
        grad_inputs[None],
        sums[0].astype(f32) * factor,
        sums[1].astype(f32) * factor,
        tap_gate,
        tap_up,
    )


def solution(mesh):
    placed = (
        P(("rep", "fs"), "tp", None),
        P(("rep", "fs"), None, "tp"),
        P(("rep", "fs"), None, "tp"),
        P(("rep", "fs"), None, "tp"),
        P("fs", "tp"),
        P("fs", "tp"),
        P(),
        P(),
    )
    return jax.shard_map(
        per_device,
        mesh=mesh,
        in_specs=placed,
        out_specs=(P(("rep", "fs"), "tp", None), P("fs", "tp"), P("fs", "tp"), P(), P()),
        check_vma=False,
    )
```

time: 536 us -> 129 us (0.24)
  waiting for transfers between devices: 418 us -> 0 us
  Pallas kernels: 0 us -> 121 us
  other arithmetic: 46.8 us -> 4.95 us
  matrix products: 29.9 us -> 0 us
  local copies, waits for them, and re-layouts: 19.1 us -> 2.39 us
  between operations: 15.4 us -> 0.66 us
  blocking collectives: 5.9 us -> 0 us
    psum x2 -> x0, waiting for transfers between devices: 218 us -> none  [the longest x1 135 us: in_one(): subtotal = lax.psum(ravelled, axis)]
    reduce_scatter x1 -> x0, waiting for transfers between devices: 198 us -> none  [side_by_side(): result = lax.psum_scatter(both, axis, scatter_dimension=dim, tiled=True)]
    pallas_call x0 -> x1, Pallas kernels: none -> 121 us  [per_device(): pl.pallas_call(kernel, out_shape=(jax.ShapeDtypeStruct((HALF, WIDTH), bf1...]
    dot_general x4 -> x0, matrix products: 29.9 us -> none  [the longest x2 17.1 us: project(): jnp.einsum('lkf,knf->ln', stacked, weight_block, preferred_element_type=j...]
    reduce_sum x3 -> x0, other arithmetic: 14 us -> none  [the longest x2 11.8 us: causal_mix(): kernel[1] * padded[1:length + 1]]
    concatenate x2 -> x0, other arithmetic: 9.78 us -> none  [the longest x1 9.14 us: side_by_side(): both = jnp.concatenate(arrays, axis=along)]
    another operation x3 -> x0, other arithmetic: 8.93 us -> none
    all_to_all x1 -> x0, blocking collectives: 5.9 us -> none  [sum_at_owner(): parts = lax.all_to_all(split_up(x, dim, count), axis, 0, 0, tiled=True)]
  transfers between devices with their start and end apart: 6 -> 0, of which waited for: 3 -> 0; matrix products, arithmetic and copies ran while one was open for 12% -> 0% of each run, Pallas kernels for 0% -> 0%
where the time goes in v1:
time: 129 us
  Pallas kernels  121 us (94%)
  other arithmetic  4.95 us (4%)
  local copies, waits for them, and re-layouts  2.39 us (2%)
    pallas_call x1, Pallas kernels, per_device(): pl.pallas_call(kernel, out_shape=(jax.ShapeDtypeStruct((HALF, WIDTH), bf1...  121 us
    mul x1, other arithmetic, per_device(): sums[1].astype(f32) * factor  4.95 us

profile of v1, /device:TPU:1, one launch (start us, length us, event | category | flops | bytes accessed | tf_op | source)
XLA Modules:
  0.0 128.8 jit_solution(9375833609020469356)
XLA Ops:
  0.6 120.8 %shard_map.119 = (bf16[384,2048]{1,0:T(8,128)(2,1)}, bf16[2,512,1408]{2,1,0:T(8,128)(2,1)}, f32[3,2816]{1,0:T(4,128)}, f32[3,2816]{1,0:T(4,128)}) custom-call(bf16[1,384,2048]{2,1,0:T(8,128)(2,1)} %x_hbm.1, bf16[1,768,1408]{2,1,0:T(8,128)(2,1)} %pg_hbm.1, bf16[1,768,1408]{2,1,0:T(8,128)(2,1)} %pu_hbm.1, bf16[1,768,1408]{2,1,0:T(8,128)(2,1)} %ct_hbm.1, ...), custom_call_target="tpu_custom_call" | custom-call | tf_op jit(solution)/shard_map/pallas_call | solution.py:491
  121.5 0.0 copy-start
  121.5 5.0 %multiply_bitcast_fusion = (f32[512,1408]{1,0:T(8,128)}, f32[512,1408]{1,0:T(8,128)}) fusion(bf16[2,512,1408]{2,1,0:T(8,128)(2,1)} %get-tuple-element.10), kind=kLoop, calls=%fused_computation | loop fusion | flops 2883584 | bytes 8650752 | tf_op jit(solution)/shard_map/mul | solution.py:510
  126.4 0.0 copy-start.2
  126.4 0.0 copy-start.1
  126.4 0.0 copy-done
  126.5 1.1 copy.16
  127.6 0.0 copy-done.2
  127.6 0.6 copy.17
  128.2 0.0 copy-done.1
  128.2 0.6 copy.18
Async XLA Ops:
  121.5 5.0 %copy-start = (bf16[384,2048]{1,0:T(8,128)(2,1)S(1)}, bf16[384,2048]{1,0:T(8,128)(2,1)}, u32[]{:S(2)}) copy-start(bf16[384,2048]{1,0:T(8,128)(2,1)} %get-tuple-element.9) | copy-start | bytes 4718596
  126.4 1.2 copy-start.2
  126.4 1.8 %copy-start.1 = (f32[3,2816]{1,0:T(4,128)S(1)}, f32[3,2816]{1,0:T(4,128)}, u32[]{:S(2)}) copy-start(f32[3,2816]{1,0:T(4,128)} %get-tuple-element.24) | copy-start | bytes 101380

commit v2 on v1

v2 whole, which is shorter than its diff:
```python
import functools

import jax
import jax.numpy as jnp
from jax import lax
from jax.experimental import pallas as pl
from jax.experimental.pallas import tpu as pltpu
from jax.sharding import PartitionSpec as P

MESH = pl.DeviceIdType.MESH
LEN = 768
COLS = 1408
WIDTH = 2048
TOKENS = 49152
SPLITS = ((0, 256), (256, 512), (768, 640))
CHUNK = 64
PAD = 16
STRIPE = 32
FAR = ((0, 128), (128, 64), (192, 64))
GROUPS = ((0, 768), (768, 640))
HALF = LEN // 2
ROOT = 0.7978845608028654
CUBIC = 0.044715
bf16, f32 = jnp.bfloat16, jnp.float32


def wrap(value, n=4):
    return lax.rem(value + 2 * n, n)


def mult(value, n):
    return pl.multiple_of(value, n)


def kernel(
    x_hbm, pg_hbm, pu_hbm, ct_hbm, wg_hbm, wu_hbm, tg_hbm, tu_hbm,
    gi_out, ag_out, tap_out,
    pg, pu, ct, xs, xt, wall, buf0, buf1, buf2, own, acc1, two0, two1, two2, acc2,
    out3_0, out3_1, out3_2, in3_0, in3_1, in3_2, ag, taps, tfin, gsend, gown, grecv, tg_ref, tu_ref,
    loc, osem, xsem, ws, w0r, w1r, w2r, w3r, w4r, p1s, p1r, p2s, p2r, p3s, p3r,
    a1s, a1r, a2s, a2r, a3s, a3r, tss, tsr, gss, gsr,
):
    rep, y, c = lax.axis_index("rep"), lax.axis_index("fs"), lax.axis_index("tp")
    z, x = rep // 4, lax.rem(rep, 4)
    first, second = (x, z), (z, x)
    bufs, twos = (buf0, buf1, buf2), (two0, two1, two2)
    outs3, ins3 = (out3_0, out3_1, out3_2), (in3_0, in3_1, in3_2)

    def dev(dx=0, dz=0, dy=0, dc=0):
        return (wrap(z + dz) * 4 + wrap(x + dx), wrap(y + dy), wrap(c + dc, 2))

    def first_dev(p, d):
        return dev(dx=d) if p == 0 else dev(dz=d)

    def second_dev(p, d):
        return dev(dz=d) if p == 0 else dev(dx=d)

    def remote(src, dst, send, recv, where):
        return pltpu.make_async_remote_copy(
            src_ref=src, dst_ref=dst, send_sem=send, recv_sem=recv, device_id=where, device_id_type=MESH
        )

    def send(src, dst, send_sem, recv_sem, where):
        remote(src, dst, send_sem, recv_sem, where).start()

    def received(place, sem):
        remote(place, place, sem, sem, dev(dc=1)).wait_recv()

    def sent(place, sem):
        remote(place, place, sem, sem, dev(dc=1)).wait_send()

    local = []

    def load(src, dst):
        copy = pltpu.make_async_copy(src, dst, loc.at[len(local)])
        copy.start()
        local.append(copy)
        return copy

    tap_loads = [load(tg_hbm, tg_ref), load(tu_hbm, tu_ref)]
    pre = []
    for at, width in SPLITS:
        cols = pl.ds(at, width)
        pre.append(
            [load(h.at[0, :, cols], v.at[pl.ds(PAD, LEN), cols]) for h, v in ((pg_hbm, pg), (pu_hbm, pu), (ct_hbm, ct))]
        )
    mine = pl.ds(mult(c * HALF, HALF), HALF)
    x_local = load(x_hbm.at[0], xs.at[mine])
    w_local = [load(h, wall.at[g, y]) for g, h in enumerate((wg_hbm, wu_hbm))]
    pg[0:PAD, :] = jnp.zeros((PAD, COLS), bf16)
    pu[0:PAD, :] = jnp.zeros((PAD, COLS), bf16)

    peers = [dev(dx=d) for d in (1, 2, 3)] + [dev(dz=d) for d in (1, 2, 3)]
    peers += [dev(dy=d) for d in (1, 2, 3)] + [dev(dc=1)]
    barrier = pltpu.get_barrier_semaphore()
    for peer in peers:
        pl.semaphore_signal(barrier, inc=1, device_id=peer, device_id_type=MESH)
    pl.semaphore_wait(barrier, len(peers))

    send(x_hbm.at[0], xs.at[mine], xsem.at[0], xsem.at[1], dev(dc=1))
    ways = ((-1, x, 0, 512 - 4 * STRIPE), (1, z, 256, 0))

    def ring_dev(way, d):
        return dev(dx=d) if way == 0 else dev(dz=d)

    def stripe(way, d):
        source, at, _, base = ways[way]
        return wrap(y + source), pl.ds(mult(base + wrap(at + d) * STRIPE, STRIPE), STRIPE)

    def passed(way):
        source, _, start, _ = ways[way]
        return wrap(y + source), pl.ds(start, 256)

    def rest(way):
        source = ways[way][0]
        return wrap(y + source), pl.ds(256 if way == 0 else 4 * STRIPE, 256 - 4 * STRIPE)

    for level, rows_of in enumerate((lambda way: stripe(way, 0), passed, rest)):
        for g, h in enumerate((wg_hbm, wu_hbm)):
            for way in range(2):
                rows = rows_of(way)[1]
                sem = w0r.at[way] if level == 0 else w1r.at[way * 2 + level - 1]
                send(h.at[rows], wall.at[g, y, rows], ws.at[0], sem, dev(dy=-ways[way][0]))

    def stripe_start():
        for way in range(2):
            shard, rows = stripe(way, 0)
            place = wall.at[:, shard, rows]
            received(place, w0r.at[way])
            for side, d in enumerate((1, -1)):
                send(place, place, ws.at[1], w3r.at[way * 2 + side], ring_dev(way, d))

    def stripe_pass():
        for way in range(2):
            for side, d in enumerate((1, -1)):
                shard, rows = stripe(way, -d)
                received(wall.at[:, shard, rows], w3r.at[way * 2 + side])
                place = wall.at[side, shard, rows]
                send(place, place, ws.at[2], w4r.at[way * 2 + side], ring_dev(way, d))

    def stripe_end():
        for way in range(2):
            shard, rows = stripe(way, 2)
            for side in range(2):
                received(wall.at[side, shard, rows], w4r.at[way * 2 + side])

    def w_arrived(way, level):
        shard, rows = (passed, rest)[level](way)
        received(wall.at[:, shard, rows], w1r.at[way * 2 + level])

    def w_forward(piece):
        at, count = FAR[piece]
        for way in range(2):
            place = wall.at[:, wrap(y + ways[way][0]), pl.ds(way * 256 + at, count)]
            send(place, place, ws.at[3], w2r.at[way * len(FAR) + piece], dev(dy=-ways[way][0]))

    def w_far_arrived(piece):
        at, count = FAR[piece]
        for way in range(2):
            received(wall.at[:, wrap(y + 2), pl.ds(way * 256 + at, count)], w2r.at[way * len(FAR) + piece])

    def elementwise(k, low, high):
        at = SPLITS[k][0]

        def column(b, _):
            col = mult(at + b * 128, 128)
            cols = pl.ds(col, 128)
            shared = pl.ds(mult(c * COLS + col, 128), 128)
            kg = tg_ref[:, shared].astype(f32)
            ku = tu_ref[:, shared].astype(f32)
            kg = [kg[j : j + 1] for j in range(3)]
            ku = [ku[j : j + 1] for j in range(3)]

            def rows(i, carry):
                next_g, next_u, sums = carry
                r = mult(LEN - CHUNK - i * CHUNK, CHUNK)
                span, here = pl.ds(r, CHUNK + PAD), pl.ds(r + PAD, CHUNK)
                eg = pg[span, cols].astype(f32)[8:]
                eu = pu[span, cols].astype(f32)[8:]
                co = ct[here, cols].astype(f32)
                sg = [pltpu.roll(eg, 2, 0)[8:], pltpu.roll(eg, 1, 0)[8:], eg[8:]]
                su = [pltpu.roll(eu, 2, 0)[8:], pltpu.roll(eu, 1, 0)[8:], eu[8:]]
                v = kg[0] * sg[0] + kg[1] * sg[1] + kg[2] * sg[2]
                m = ku[0] * su[0] + ku[1] * su[1] + ku[2] * su[2]
                v2 = v * v
                t = jnp.tanh(v * (ROOT + (ROOT * CUBIC) * v2))
                h = 0.5 + 0.5 * t
                slope = h * (1.0 + v * (1.0 - t) * (ROOT + (3.0 * ROOT * CUBIC) * v2))
                bg = co * m * slope
                bu = co * (v * h)
                new = tuple(
                    s + (back * moved).reshape(CHUNK // 8, 8, 128).sum(0)
                    for s, (back, moved) in zip(sums, [(bg, q) for q in sg] + [(bu, q) for q in su])
                )
                for ref, back, after, taps_of in ((pg, bg, next_g, kg), (pu, bu, next_u, ku)):
                    whole = jnp.concatenate([back, after], axis=0)
                    one = pltpu.roll(whole, CHUNK + 7, 0)[:CHUNK]
                    two = pltpu.roll(whole, CHUNK + 6, 0)[:CHUNK]
                    ref[here, cols] = (taps_of[2] * back + taps_of[1] * one + taps_of[0] * two).astype(bf16)
                return bg[:8], bu[:8], new

            zero = jnp.zeros((8, 128), f32)
            _, _, sums = lax.fori_loop(0, LEN // CHUNK, rows, (zero, zero, (zero,) * 6))
            rows8 = [jnp.sum(s, axis=0, keepdims=True) for s in sums]
            taps[0, x, :, cols] = jnp.concatenate(rows8 + [jnp.zeros((2, 128), f32)], axis=0)
            return 0

        lax.fori_loop(low, high, column, 0)

    grads = (pg, pu)

    def own_rows(p, s):
        parts = []
        for yb in range(4):
            chunk = wrap(first[p] - 1 - s) if yb < 2 else wrap(first[p] + 1 + s)
            parts.append(xt[pl.ds(mult(yb * 512 + chunk * 128, 128), 128), :])
        return jnp.concatenate(parts, axis=0)

    def product(p, k, s):
        at, width = SPLITS[k]
        right = grads[p][PAD : PAD + LEN, at : at + width]
        return jnp.dot(own_rows(p, s), right, preferred_element_type=f32).reshape(4, 128, width)

    def p1_send(k, p, s):
        for way in range(2):
            pair = pl.ds(way * 2, 2)
            send(
                bufs[k].at[p, s, pair], bufs[k].at[p, s + 1, pair], p1s.at[k * 2 + p], p1r.at[(k * 2 + p) * 3 + s],
                first_dev(p, 1 - 2 * way),
            )

    def step0(k):
        for p in range(2):
            bufs[k][p, 0] = product(p, k, 0).astype(bf16)
            p1_send(k, p, 0)

    def step1(k, s):
        at, width = SPLITS[k]
        for p in range(2):
            own[p, :, :, 0:width] = product(p, k, s)
        for p in range(2):
            received(bufs[k].at[p, s], p1r.at[(k * 2 + p) * 3 + s - 1])

            def add(yb, _):
                total = bufs[k][p, s, yb].astype(f32) + own[p, yb, :, 0:width]
                if s < 3:
                    bufs[k][p, s, yb] = total.astype(bf16)
                else:
                    acc1[p, yb, :, at : at + width] = total
                return 0

            lax.fori_loop(0, 4, add, 0)
            if s < 3:
                p1_send(k, p, s)

    def p2_send(k, p, s):
        for way in range(2):
            pair = pl.ds(way * 2, 2)
            send(
                twos[k].at[p, s, pair], twos[k].at[p, s + 1, pair], p2s.at[k * 2 + p], p2r.at[(k * 2 + p) * 3 + s],
                second_dev(p, 1 - 2 * way),
            )

    def step2(k, s):
        at, width = SPLITS[k]
        for p in range(2):
            if s > 0:
                received(twos[k].at[p, s], p2r.at[(k * 2 + p) * 3 + s - 1])

            def add(yb, _):
                move = (1 - 2 * (yb // 2)) * (1 + s)
                chunk = wrap(second[p] - move)
                total = acc1[p, yb, pl.ds(mult(chunk * 32, 32), 32), at : at + width]
                if s > 0:
                    total = total + twos[k][p, s, yb].astype(f32)
                if s < 3:
                    twos[k][p, s, yb] = total.astype(bf16)
                else:
                    acc2[p, yb, :, at : at + width] = total
                return 0

            lax.fori_loop(0, 4, add, 0)
            if s < 3:
                p2_send(k, p, s)

    def p3_send(k):
        at, width = SPLITS[k]
        for p in range(2):
            for d in (1, 3, 2):
                outs3[k][p, d - 1] = acc2[p, wrap(y + d), :, at : at + width].astype(bf16)
                send(
                    outs3[k].at[p, d - 1], ins3[k].at[p, d - 1], p3s.at[k * 2 + p], p3r.at[k * 2 + p], dev(dy=d)
                )

    def block(p, group, d_first, d_second, skip=0, rows=32):
        start = wrap(first[p] + d_first) * 128 + wrap(second[p] + d_second) * 32 + skip
        at, width = GROUPS[group]
        return ag.at[p, pl.ds(mult(start, 16), rows), pl.ds(at, width)]

    def amount(p, group, rows):
        at, width = GROUPS[group]
        return ag.at[p, pl.ds(0, rows), pl.ds(at, width)]

    def p3_finish(k, p):
        at, width = SPLITS[k]
        received(ins3[k].at[p], p3r.at[k * 2 + p])
        total = acc2[p, y, :, at : at + width]
        for d in (1, 3, 2):
            total = total + ins3[k][p, d - 1].astype(f32)
        start = mult(first[p] * 128 + second[p] * 32, 32)
        ag[p, pl.ds(start, 32), at : at + width] = total.astype(bf16)

    def a1_start(group, p):
        for d in (1, 3, 2):
            index = (group * 2 + p) * 3 + d - 1
            place = block(p, group, 0, 0)
            send(place, place, a1s.at[group * 2 + p], a1r.at[index], second_dev(p, d))

    def a1_wait(group, p, d):
        received(block(p, group, 0, -d), a1r.at[(group * 2 + p) * 3 + d - 1])

    def a2_start(group, p, d):
        place = block(p, group, 0, -d)
        for way in range(2):
            send(place, place, a2s.at[group * 2 + p], a2r.at[(group * 2 + p) * 4 + d], first_dev(p, 1 - 2 * way))

    def a2_pass_on(group, p, d):
        received(amount(p, group, 64), a2r.at[(group * 2 + p) * 4 + d])
        for way in range(2):
            from_ = 2 * way - 1
            part = block(p, group, from_, -d, 16 * way, 16)
            send(part, part, a3s.at[group * 2 + p], a3r.at[group * 2 + p], first_dev(p, -from_))

    def a3_wait(group, p):
        received(amount(p, group, 128), a3r.at[group * 2 + p])
        at, width = GROUPS[group]
        cols = pl.ds(at, width)
        pltpu.make_async_copy(ag.at[p, :, cols], ag_out.at[p, :, cols], osem.at[1]).start()

    coords = (x, z, y)

    def tap_dev(stage, d):
        return dev(dx=d) if stage == 0 else dev(dz=d) if stage == 1 else dev(dy=d)

    def tap_send(stage):
        place = taps.at[stage, coords[stage]]
        for d in (1, 2, 3):
            send(place, place, tss.at[stage], tsr.at[stage], tap_dev(stage, d))

    def tap_sum(stage):
        received(taps.at[stage, 0:3], tsr.at[stage])
        total = taps[stage, 0] + taps[stage, 1] + taps[stage, 2] + taps[stage, 3]
        if stage < 2:
            taps[stage + 1, coords[stage + 1]] = total
            tap_send(stage + 1)
        else:
            tfin[c] = total * (float(TOKENS) ** -0.5)
            send(tfin.at[c], tfin.at[c], tss.at[3], tsr.at[3], dev(dc=1))

    def tap_end():
        other = tfin.at[wrap(c + 1, 2)]
        received(other, tsr.at[3])
        pltpu.make_async_copy(tfin, tap_out, osem.at[2]).start()

    def project(unit, d, starts):
        shard = wrap(y + d)

        def weights(g):
            return jnp.concatenate([wall[g, shard, at : at + 128, :] for at in starts], axis=0)

        def side(which, _):
            to_partner = 1 - which
            row = mult(PAD + wrap(c + to_partner, 2) * HALF, 16)
            dims = (((1,), (1,)), ((), ()))
            value = lax.dot_general(pg[pl.ds(row, HALF), :], weights(0), dims, preferred_element_type=f32)
            value = value + lax.dot_general(pu[pl.ds(row, HALF), :], weights(1), dims, preferred_element_type=f32)
            gsend[which, unit] = value.astype(bf16)
            return 0

        lax.fori_loop(0, 2, side, 0)
        send(gsend.at[0, unit], grecv.at[unit], gss.at[0], gsr.at[unit], dev(dc=1))

    def combine(unit, d, starts):
        received(grecv.at[unit], gsr.at[unit])
        gown[unit] = (gsend[1, unit].astype(f32) + grecv[unit].astype(f32)).astype(bf16)
        for i, at in enumerate(starts):
            col = mult(wrap(y + d) * 512 + at, 128)
            part = gown.at[unit, :, pl.ds(i * 128, 128)]
            pltpu.make_async_copy(part, gi_out.at[:, pl.ds(col, 128)], osem.at[0]).start()

    def turn_half(side, count, block_of):
        rows = pl.ds(mult(side * HALF, HALF), HALF)

        def turn(i, _):
            at = pl.ds(mult(block_of(i) * 128, 128), 128)
            xt[at, rows] = xs[rows, at].T
            return 0

        lax.fori_loop(0, count, turn, 0)

    def early(i):
        yb = lax.rem(i, 4)
        base = jnp.where(i < 4, x, z)
        return yb * 4 + wrap(base - 1 + 2 * (yb // 2))

    def late(i):
        yb = i // 3
        return yb * 4 + wrap(x + lax.rem(i, 3) + 2 * (yb // 2))

    for copy in tap_loads + pre[0]:
        copy.wait()
    elementwise(0, 0, 2)
    x_local.wait()
    turn_half(c, 8, early)
    other_half = xs.at[pl.ds(mult(wrap(c + 1, 2) * HALF, HALF), HALF)]
    received(other_half, xsem.at[1])
    turn_half(wrap(c + 1, 2), 8, early)
    units = [(0, (0, 128)), (0, (256, 384)), (-1, (0, 128)), (1, (256, 384)), (-1, (256, 384)), (1, (0, 128))]
    units += [(2, (0, 256)), (2, (128, 384))]
    step0(0)
    for copy in pre[1]:
        copy.wait()
    elementwise(1, 0, 2)
    stripe_start()
    elementwise(1, 2, 4)
    step0(1)
    turn_half(0, 12, late)
    turn_half(1, 12, late)
    step1(0, 1)
    for copy in pre[2]:
        copy.wait()
    elementwise(2, 0, 2)
    stripe_pass()
    elementwise(2, 2, 5)
    step0(2)
    tap_send(0)
    step1(1, 1)
    step1(0, 2)
    for copy in w_local:
        copy.wait()
    step1(2, 1)
    project(0, *units[0])
    step1(1, 2)
    step1(0, 3)
    step2(0, 0)
    tap_sum(0)
    project(1, *units[1])
    step1(2, 2)
    for way in range(2):
        w_arrived(way, 0)
    w_forward(0)
    w_forward(1)
    project(2, *units[2])
    step1(1, 3)
    step2(1, 0)
    step2(0, 1)
    combine(0, *units[0])
    combine(1, *units[1])
    project(3, *units[3])
    step1(2, 3)
    step2(2, 0)
    step2(1, 1)
    step2(0, 2)
    tap_sum(1)
    step2(2, 1)
    step2(1, 2)
    step2(0, 3)
    p3_send(0)
    step2(2, 2)
    step2(1, 3)
    p3_send(1)
    step2(2, 3)
    p3_send(2)
    w_forward(2)
    stripe_end()
    for way in range(2):
        w_arrived(way, 1)
    project(4, *units[4])
    for p in range(2):
        for k in range(2):
            p3_finish(k, p)
        a1_start(0, p)
        a2_start(0, p, 0)
    combine(2, *units[2])
    combine(3, *units[3])
    for p in range(2):
        p3_finish(2, p)
        a1_start(1, p)
        a2_start(1, p, 0)
    for group in range(2):
        for d in (1, 3, 2):
            for p in range(2):
                a1_wait(group, p, d)
                a2_start(group, p, d)
    project(5, *units[5])
    tap_sum(2)
    for group in range(2):
        for d in (0, 1, 3, 2):
            for p in range(2):
                a2_pass_on(group, p, d)
    w_far_arrived(0)
    project(6, *units[6])
    combine(4, *units[4])
    combine(5, *units[5])
    tap_end()
    for p in range(2):
        a3_wait(0, p)
    w_far_arrived(1)
    w_far_arrived(2)
    project(7, *units[7])
    for p in range(2):
        a3_wait(1, p)
    combine(6, *units[6])
    sent(xs.at[mine], xsem.at[0])
    sent(wall.at[:, 0:2, 0 : 512 - 3 * STRIPE], ws.at[0])
    sent(wall.at[:, 0, 0 : 4 * STRIPE], ws.at[1])
    sent(wall.at[0, 0, 0 : 4 * STRIPE], ws.at[2])
    sent(wall.at[:, 0], ws.at[3])
    for k in range(len(SPLITS)):
        for p in range(2):
            sent(bufs[k].at[p, 0:3], p1s.at[k * 2 + p])
            sent(twos[k].at[p, 0:3], p2s.at[k * 2 + p])
            sent(outs3[k].at[p], p3s.at[k * 2 + p])
    for group in range(2):
        for p in range(2):
            sent(amount(p, group, 96), a1s.at[group * 2 + p])
            sent(amount(p, group, 256), a2s.at[group * 2 + p])
            sent(amount(p, group, 128), a3s.at[group * 2 + p])
    for stage in range(3):
        sent(taps.at[stage, 0:3], tss.at[stage])
    sent(tfin.at[0], tss.at[3])
    sent(gsend.at[0], gss.at[0])
    combine(7, *units[7])
    for sem, ref in enumerate((gown, ag, tfin)):
        pltpu.make_async_copy(ref, ref, osem.at[sem]).wait()


def finish(gi_in, ag_in, tap_in, gi_out, gate_out, up_out, tap_gate, tap_up, gi, half, full, tap, tg, tu, sems):
    copies, count = [], 8
    rows = 512 // count

    def start(src, dst):
        copy = pltpu.make_async_copy(src, dst, sems.at[len(copies)])
        copy.start()
        copies.append(copy)
        return copy

    tap_load = start(tap_in, tap)
    loads = []
    for i in range(count):
        part = pl.ds(i * rows, rows)
        loads.append(start(ag_in.at[:, part], half.at[:, part]))
    gi_load = start(gi_in, gi)
    tap_load.wait()
    for side in range(2):
        cols = slice(side * COLS, side * COLS + COLS)
        tg[:, cols] = tap[side, 0:3]
        tu[:, cols] = tap[side, 3:6]
    stores = [start(tg, tap_gate), start(tu, tap_up)]
    for i in range(count):
        part = pl.ds(i * rows, rows)
        loads[i].wait()
        for p, target in enumerate((gate_out, up_out)):
            full[p, part] = half[p, part].astype(f32) * (float(TOKENS) ** -0.5)
            stores.append(start(full.at[p, part], target.at[part]))
    gi_load.wait()
    stores.append(start(gi, gi_out.at[0]))
    for copy in stores:
        copy.wait()


def per_device(inputs, pre_gate, pre_up, cotangent, w_gate, w_up, taps_gate, taps_up):
    any_ = pl.BlockSpec(memory_space=pl.ANY)
    dma = pltpu.SemaphoreType.DMA
    widths = [width for _, width in SPLITS]
    count = len(widths)
    scratch = (
        [pltpu.VMEM((PAD + LEN, COLS), bf16)] * 3
        + [pltpu.VMEM((LEN, WIDTH), bf16), pltpu.VMEM((WIDTH, LEN), bf16), pltpu.VMEM((2, 4, 512, COLS), bf16)]
        + [pltpu.VMEM((2, 4, 4, 128, width), bf16) for width in widths]
        + [pltpu.VMEM((2, 4, 128, max(widths)), f32), pltpu.VMEM((2, 4, 128, COLS), f32)]
        + [pltpu.VMEM((2, 4, 4, 32, width), bf16) for width in widths]
        + [pltpu.VMEM((2, 4, 32, COLS), f32)]
        + [pltpu.VMEM((2, 3, 32, width), bf16) for width in widths] * 2
        + [pltpu.VMEM((2, 512, COLS), bf16), pltpu.VMEM((3, 4, 8, COLS), f32), pltpu.VMEM((2, 8, COLS), f32)]
        + [pltpu.VMEM((2, 8, HALF, 256), bf16), pltpu.VMEM((8, HALF, 256), bf16), pltpu.VMEM((8, HALF, 256), bf16)]
        + [pltpu.VMEM((3, 2 * COLS), bf16)] * 2
        + [dma((14,)), dma((3,)), dma((2,)), dma((4,)), dma((2,)), dma((4,)), dma((2 * len(FAR),)), dma((4,)), dma((4,))]
        + [dma((2 * count,)), dma((6 * count,))] * 2
        + [dma((2 * count,)), dma((2 * count,))]
        + [dma((4,)), dma((12,)), dma((4,)), dma((16,)), dma((4,)), dma((4,)), dma((4,)), dma((4,)), dma((1,)), dma((8,))]
    )
    grad_inputs, sums, tap_sums = pl.pallas_call(
        kernel,
        out_shape=(
            jax.ShapeDtypeStruct((HALF, WIDTH), bf16),
            jax.ShapeDtypeStruct((2, 512, COLS), bf16),
            jax.ShapeDtypeStruct((2, 8, COLS), f32),
        ),
        in_specs=[any_] * 8,
        out_specs=(any_,) * 3,
        scratch_shapes=scratch,
        compiler_params=pltpu.CompilerParams(
            collective_id=0, has_side_effects=True, vmem_limit_bytes=67043328
        ),
    )(inputs, pre_gate, pre_up, cotangent, w_gate, w_up, taps_gate, taps_up)
    return tuple(
        pl.pallas_call(
            finish,
            out_shape=(
                jax.ShapeDtypeStruct((1, HALF, WIDTH), bf16),
                jax.ShapeDtypeStruct((512, COLS), f32),
                jax.ShapeDtypeStruct((512, COLS), f32),
                jax.ShapeDtypeStruct((3, 2 * COLS), f32),
                jax.ShapeDtypeStruct((3, 2 * COLS), f32),
            ),
            in_specs=[any_] * 3,
            out_specs=(any_,) * 5,
            scratch_shapes=[
                pltpu.VMEM((HALF, WIDTH), bf16),
                pltpu.VMEM((2, 512, COLS), bf16),
                pltpu.VMEM((2, 512, COLS), f32),
                pltpu.VMEM((2, 8, COLS), f32),
                pltpu.VMEM((3, 2 * COLS), f32),
                pltpu.VMEM((3, 2 * COLS), f32),
                dma((32,)),
            ],
            compiler_params=pltpu.CompilerParams(vmem_limit_bytes=67043328),
        )(grad_inputs, sums, tap_sums)
    )


def solution(mesh):
    placed = (
        P(("rep", "fs"), "tp", None),
        P(("rep", "fs"), None, "tp"),
        P(("rep", "fs"), None, "tp"),
        P(("rep", "fs"), None, "tp"),
        P("fs", "tp"),
        P("fs", "tp"),
        P(),
        P(),
    )
    return jax.shard_map(
        per_device,
        mesh=mesh,
        in_specs=placed,
        out_specs=(P(("rep", "fs"), "tp", None), P("fs", "tp"), P("fs", "tp"), P(), P()),
        check_vma=False,
    )
```

time: 129 us -> 117 us (0.907)
  Pallas kernels: 121 us -> 116 us
  other arithmetic: 4.95 us -> 0 us
  local copies, waits for them, and re-layouts: 2.39 us -> 0 us
    pallas_call x1, Pallas kernels: 121 us -> 111 us  [per_device(): pl.pallas_call(kernel, out_shape=(jax.ShapeDtypeStruct((HALF, WIDTH), bf1...]
    mul x1 -> x0, other arithmetic: 4.95 us -> none  [per_device(): sums[1].astype(f32) * factor]
    pallas_call x0 -> x1, Pallas kernels: none -> 4.62 us  [per_device(): pl.pallas_call(finish, out_shape=(jax.ShapeDtypeStruct((1, HALF, WIDTH),...]
    unnamed x9 -> x0, local copies, waits for them, and re-layouts: 2.39 us -> none
where the time goes in v2:
time: 117 us
  Pallas kernels  116 us (99%)
    pallas_call x1, Pallas kernels, per_device(): pl.pallas_call(kernel, out_shape=(jax.ShapeDtypeStruct((HALF, WIDTH), bf1...  111 us
    pallas_call x1, Pallas kernels, per_device(): pl.pallas_call(finish, out_shape=(jax.ShapeDtypeStruct((1, HALF, WIDTH),...  4.62 us

profile of v2, /device:TPU:1, one launch (start us, length us, event | category | flops | bytes accessed | tf_op | source)
XLA Modules:
  0.0 116.9 jit_solution(12959533601008950740)
XLA Ops:
  0.6 111.5 %shard_map.119 = (bf16[384,2048]{1,0:T(8,128)(2,1)}, bf16[2,512,1408]{2,1,0:T(8,128)(2,1)}, f32[2,8,1408]{2,1,0:T(8,128)}) custom-call(bf16[1,384,2048]{2,1,0:T(8,128)(2,1)} %x_hbm.1, bf16[1,768,1408]{2,1,0:T(8,128)(2,1)} %pg_hbm.1, bf16[1,768,1408]{2,1,0:T(8,128)(2,1)} %pu_hbm.1, bf16[1,768,1408]{2,1,0:T(8,128)(2,1)} %ct_hbm.1, bf16[512,1408]{1,0:T(8,128)(2,1)} %wg_hbm.1, ...), custom_call_target="tpu_custom_call" | custom-call | tf_op jit(solution)/shard_map/pallas_call | solution.py:593
  112.1 4.6 %shard_map.120 = (bf16[1,384,2048]{2,1,0:T(8,128)(2,1)}, f32[512,1408]{1,0:T(8,128)}, f32[512,1408]{1,0:T(8,128)}, f32[3,2816]{1,0:T(4,128)}, f32[3,2816]{1,0:T(4,128)}) custom-call(bf16[384,2048]{1,0:T(8,128)(2,1)} %get-tuple-element.8.gi_in, bf16[2,512,1408]{2,1,0:T(8,128)(2,1)} %get-tuple-element.9.ag_in, f32[2,8,1408]{2,1,0:T(8,128)} %get-tuple-element.10.tap_in), custom_call_target="tpu_custom_call" | custom-call | tf_op jit(solution)/shard_map/pallas_call | solution.py:608

commit v3 on v2

--- a/solution.py
+++ b/solution.py
@@ -16,7 +16,7 @@
 CHUNK = 64
 PAD = 16
 STRIPE = 32
-FAR = ((0, 128), (128, 64), (192, 64))
+FAR = ((0, 128), (128, 32), (160, 32), (192, 64))
 GROUPS = ((0, 768), (768, 640))
 HALF = LEN // 2
 ROOT = 0.7978845608028654
@@ -433,35 +433,38 @@
     stripe_pass()
     elementwise(2, 2, 5)
     step0(2)
-    tap_send(0)
     step1(1, 1)
     step1(0, 2)
     for copy in w_local:
         copy.wait()
+    project(0, *units[0])
+    project(1, *units[1])
     step1(2, 1)
-    project(0, *units[0])
     step1(1, 2)
-    step1(0, 3)
-    step2(0, 0)
-    tap_sum(0)
-    project(1, *units[1])
-    step1(2, 2)
     for way in range(2):
         w_arrived(way, 0)
     w_forward(0)
-    w_forward(1)
     project(2, *units[2])
+    step1(0, 3)
+    step2(0, 0)
+    project(3, *units[3])
+    step1(2, 2)
+    combine(0, *units[0])
+    combine(1, *units[1])
     step1(1, 3)
     step2(1, 0)
     step2(0, 1)
-    combine(0, *units[0])
-    combine(1, *units[1])
-    project(3, *units[3])
+    stripe_end()
+    for way in range(2):
+        w_arrived(way, 1)
+    project(4, *units[4])
+    combine(2, *units[2])
+    combine(3, *units[3])
     step1(2, 3)
     step2(2, 0)
+    w_forward(1)
     step2(1, 1)
     step2(0, 2)
-    tap_sum(1)
     step2(2, 1)
     step2(1, 2)
     step2(0, 3)
@@ -471,46 +474,48 @@
     p3_send(1)
     step2(2, 3)
     p3_send(2)
+    tap_send(0)
     w_forward(2)
-    stripe_end()
-    for way in range(2):
-        w_arrived(way, 1)
-    project(4, *units[4])
+    w_forward(3)
+    project(5, *units[5])
     for p in range(2):
         for k in range(2):
             p3_finish(k, p)
         a1_start(0, p)
         a2_start(0, p, 0)
-    combine(2, *units[2])
-    combine(3, *units[3])
     for p in range(2):
         p3_finish(2, p)
         a1_start(1, p)
         a2_start(1, p, 0)
-    for group in range(2):
-        for d in (1, 3, 2):
-            for p in range(2):
-                a1_wait(group, p, d)
-                a2_start(group, p, d)
-    project(5, *units[5])
-    tap_sum(2)
-    for group in range(2):
-        for d in (0, 1, 3, 2):
-            for p in range(2):
-                a2_pass_on(group, p, d)
+    tap_sum(0)
     w_far_arrived(0)
+    for d in (1, 3, 2):
+        for p in range(2):
+            a1_wait(0, p, d)
+            a2_start(0, p, d)
     project(6, *units[6])
+    for d in (1, 3, 2):
+        for p in range(2):
+            a1_wait(1, p, d)
+            a2_start(1, p, d)
+    tap_sum(1)
     combine(4, *units[4])
     combine(5, *units[5])
+    for d in (0, 1, 3, 2):
+        for p in range(2):
+            a2_pass_on(0, p, d)
+    tap_sum(2)
+    for d in (0, 1, 3, 2):
+        for p in range(2):
+            a2_pass_on(1, p, d)
+    for piece in range(1, len(FAR)):
+        w_far_arrived(piece)
+    project(7, *units[7])
+    combine(6, *units[6])
     tap_end()
-    for p in range(2):
-        a3_wait(0, p)
-    w_far_arrived(1)
-    w_far_arrived(2)
-    project(7, *units[7])
-    for p in range(2):
-        a3_wait(1, p)
-    combine(6, *units[6])
+    for group in range(2):
+        for p in range(2):
+            a3_wait(group, p)
     sent(xs.at[mine], xsem.at[0])
     sent(wall.at[:, 0:2, 0 : 512 - 3 * STRIPE], ws.at[0])
     sent(wall.at[:, 0, 0 : 4 * STRIPE], ws.at[1])

time: 117 us -> 112 us (0.957)
  Pallas kernels: 116 us -> 111 us
    pallas_call x1, Pallas kernels: 111 us -> 107 us  [per_device(): pl.pallas_call(kernel, out_shape=(jax.ShapeDtypeStruct((HALF, WIDTH), bf1...]
where the time goes in v3:
time: 112 us
  Pallas kernels  111 us (99%)
    pallas_call x1, Pallas kernels, per_device(): pl.pallas_call(kernel, out_shape=(jax.ShapeDtypeStruct((HALF, WIDTH), bf1...  107 us
    pallas_call x1, Pallas kernels, per_device(): pl.pallas_call(finish, out_shape=(jax.ShapeDtypeStruct((1, HALF, WIDTH),...  4.62 us

profile of v3, /device:TPU:1, one launch (start us, length us, event | category | flops | bytes accessed | tf_op | source)
XLA Modules:
  0.0 112.0 jit_solution(12734013310887027083)
XLA Ops:
  0.6 106.6 %shard_map.119 = (bf16[384,2048]{1,0:T(8,128)(2,1)}, bf16[2,512,1408]{2,1,0:T(8,128)(2,1)}, f32[2,8,1408]{2,1,0:T(8,128)}) custom-call(bf16[1,384,2048]{2,1,0:T(8,128)(2,1)} %x_hbm.1, bf16[1,768,1408]{2,1,0:T(8,128)(2,1)} %pg_hbm.1, bf16[1,768,1408]{2,1,0:T(8,128)(2,1)} %pu_hbm.1, bf16[1,768,1408]{2,1,0:T(8,128)(2,1)} %ct_hbm.1, bf16[512,1408]{1,0:T(8,128)(2,1)} %wg_hbm.1, ...), custom_call_target="tpu_custom_call" | custom-call | tf_op jit(solution)/shard_map/pallas_call | solution.py:598
  107.2 4.6 %shard_map.120 = (bf16[1,384,2048]{2,1,0:T(8,128)(2,1)}, f32[512,1408]{1,0:T(8,128)}, f32[512,1408]{1,0:T(8,128)}, f32[3,2816]{1,0:T(4,128)}, f32[3,2816]{1,0:T(4,128)}) custom-call(bf16[384,2048]{1,0:T(8,128)(2,1)} %get-tuple-element.8.gi_in, bf16[2,512,1408]{2,1,0:T(8,128)(2,1)} %get-tuple-element.9.ag_in, f32[2,8,1408]{2,1,0:T(8,128)} %get-tuple-element.10.tap_in), custom_call_target="tpu_custom_call" | custom-call | tf_op jit(solution)/shard_map/pallas_call | solution.py:613

commit v4 on v3

--- a/solution.py
+++ b/solution.py
@@ -17,7 +17,7 @@
 PAD = 16
 STRIPE = 32
 FAR = ((0, 128), (128, 32), (160, 32), (192, 64))
-GROUPS = ((0, 768), (768, 640))
+GROUPS = SPLITS
 HALF = LEN // 2
 ROOT = 0.7978845608028654
 CUBIC = 0.044715
@@ -225,7 +225,7 @@
         for way in range(2):
             pair = pl.ds(way * 2, 2)
             send(
-                bufs[k].at[p, s, pair], bufs[k].at[p, s + 1, pair], p1s.at[k * 2 + p], p1r.at[(k * 2 + p) * 3 + s],
+                bufs[k].at[p, s, pair], bufs[k].at[p, s + 1, pair], p1s.at[k], p1r.at[(k * 2 + p) * 3 + s],
                 first_dev(p, 1 - 2 * way),
             )
 
@@ -257,7 +257,7 @@
         for way in range(2):
             pair = pl.ds(way * 2, 2)
             send(
-                twos[k].at[p, s, pair], twos[k].at[p, s + 1, pair], p2s.at[k * 2 + p], p2r.at[(k * 2 + p) * 3 + s],
+                twos[k].at[p, s, pair], twos[k].at[p, s + 1, pair], p2s.at[k], p2r.at[(k * 2 + p) * 3 + s],
                 second_dev(p, 1 - 2 * way),
             )
 
@@ -289,7 +289,7 @@
             for d in (1, 3, 2):
                 outs3[k][p, d - 1] = acc2[p, wrap(y + d), :, at : at + width].astype(bf16)
                 send(
-                    outs3[k].at[p, d - 1], ins3[k].at[p, d - 1], p3s.at[k * 2 + p], p3r.at[k * 2 + p], dev(dy=d)
+                    outs3[k].at[p, d - 1], ins3[k].at[p, d - 1], p3s.at[k], p3r.at[k], dev(dy=d)
                 )
 
     def block(p, group, d_first, d_second, skip=0, rows=32):
@@ -297,13 +297,15 @@
         at, width = GROUPS[group]
         return ag.at[p, pl.ds(mult(start, 16), rows), pl.ds(at, width)]
 
-    def amount(p, group, rows):
+    def amount(group, rows):
         at, width = GROUPS[group]
-        return ag.at[p, pl.ds(0, rows), pl.ds(at, width)]
+        return ag.at[:, pl.ds(0, rows), pl.ds(at, width)]
+
+    def p3_wait(k):
+        received(ins3[k], p3r.at[k])
 
     def p3_finish(k, p):
         at, width = SPLITS[k]
-        received(ins3[k].at[p], p3r.at[k * 2 + p])
         total = acc2[p, y, :, at : at + width]
         for d in (1, 3, 2):
             total = total + ins3[k][p, d - 1].astype(f32)
@@ -312,30 +314,47 @@
 
     def a1_start(group, p):
         for d in (1, 3, 2):
-            index = (group * 2 + p) * 3 + d - 1
             place = block(p, group, 0, 0)
-            send(place, place, a1s.at[group * 2 + p], a1r.at[index], second_dev(p, d))
-
-    def a1_wait(group, p, d):
-        received(block(p, group, 0, -d), a1r.at[(group * 2 + p) * 3 + d - 1])
+            send(place, place, a1s.at[0], a1r.at[group * 3 + d - 1], second_dev(p, d))
+
+    def a1_wait(group, d):
+        received(amount(group, 32), a1r.at[group * 3 + d - 1])
 
     def a2_start(group, p, d):
         place = block(p, group, 0, -d)
         for way in range(2):
-            send(place, place, a2s.at[group * 2 + p], a2r.at[(group * 2 + p) * 4 + d], first_dev(p, 1 - 2 * way))
-
-    def a2_pass_on(group, p, d):
-        received(amount(p, group, 64), a2r.at[(group * 2 + p) * 4 + d])
-        for way in range(2):
-            from_ = 2 * way - 1
-            part = block(p, group, from_, -d, 16 * way, 16)
-            send(part, part, a3s.at[group * 2 + p], a3r.at[group * 2 + p], first_dev(p, -from_))
-
-    def a3_wait(group, p):
-        received(amount(p, group, 128), a3r.at[group * 2 + p])
+            send(place, place, a2s.at[0], a2r.at[group * 4 + d], first_dev(p, 1 - 2 * way))
+
+    def a2_pass_on(group, d):
+        received(amount(group, 64), a2r.at[group * 4 + d])
+        for p in range(2):
+            for way in range(2):
+                from_ = 2 * way - 1
+                part = block(p, group, from_, -d, 16 * way, 16)
+                send(part, part, a3s.at[0], a3r.at[group], first_dev(p, -from_))
+
+    def a3_wait(group):
+        received(amount(group, 128), a3r.at[group])
+        rows_out(group, 2)
+
+    def rows_out(group, d):
         at, width = GROUPS[group]
-        cols = pl.ds(at, width)
-        pltpu.make_async_copy(ag.at[p, :, cols], ag_out.at[p, :, cols], osem.at[1]).start()
+        for p in range(2):
+            part = p, pl.ds(mult(wrap(first[p] + d) * 128, 128), 128), pl.ds(at, width)
+            pltpu.make_async_copy(ag.at[part], ag_out.at[part], osem.at[1]).start()
+
+    def gather_start(group):
+        p3_wait(group)
+        for p in range(2):
+            p3_finish(group, p)
+            a1_start(group, p)
+            a2_start(group, p, 0)
+
+    def gather_second(group):
+        for d in (1, 3, 2):
+            a1_wait(group, d)
+            for p in range(2):
+                a2_start(group, p, d)
 
     coords = (x, z, y)
 
@@ -343,12 +362,12 @@
         return dev(dx=d) if stage == 0 else dev(dz=d) if stage == 1 else dev(dy=d)
 
     def tap_send(stage):
-        place = taps.at[stage, coords[stage]]
+        place = taps.at[stage, coords[stage], 0:6]
         for d in (1, 2, 3):
             send(place, place, tss.at[stage], tsr.at[stage], tap_dev(stage, d))
 
     def tap_sum(stage):
-        received(taps.at[stage, 0:3], tsr.at[stage])
+        received(taps.at[stage, 0:3, 0:6], tsr.at[stage])
         total = taps[stage, 0] + taps[stage, 1] + taps[stage, 2] + taps[stage, 3]
         if stage < 2:
             taps[stage + 1, coords[stage + 1]] = total
@@ -477,62 +496,45 @@
     tap_send(0)
     w_forward(2)
     w_forward(3)
+    gather_start(0)
     project(5, *units[5])
-    for p in range(2):
-        for k in range(2):
-            p3_finish(k, p)
-        a1_start(0, p)
-        a2_start(0, p, 0)
-    for p in range(2):
-        p3_finish(2, p)
-        a1_start(1, p)
-        a2_start(1, p, 0)
+    gather_start(1)
+    gather_second(0)
+    gather_start(2)
     tap_sum(0)
     w_far_arrived(0)
-    for d in (1, 3, 2):
-        for p in range(2):
-            a1_wait(0, p, d)
-            a2_start(0, p, d)
+    gather_second(1)
     project(6, *units[6])
-    for d in (1, 3, 2):
-        for p in range(2):
-            a1_wait(1, p, d)
-            a2_start(1, p, d)
+    gather_second(2)
     tap_sum(1)
     combine(4, *units[4])
     combine(5, *units[5])
-    for d in (0, 1, 3, 2):
-        for p in range(2):
-            a2_pass_on(0, p, d)
-    tap_sum(2)
-    for d in (0, 1, 3, 2):
-        for p in range(2):
-            a2_pass_on(1, p, d)
+    for group in range(3):
+        for d in (0, 1, 3, 2):
+            a2_pass_on(group, d)
+        for d in (0, -1, 1):
+            rows_out(group, d)
     for piece in range(1, len(FAR)):
         w_far_arrived(piece)
+    tap_sum(2)
     project(7, *units[7])
     combine(6, *units[6])
+    for group in range(3):
+        a3_wait(group)
     tap_end()
-    for group in range(2):
-        for p in range(2):
-            a3_wait(group, p)
     sent(xs.at[mine], xsem.at[0])
     sent(wall.at[:, 0:2, 0 : 512 - 3 * STRIPE], ws.at[0])
     sent(wall.at[:, 0, 0 : 4 * STRIPE], ws.at[1])
     sent(wall.at[0, 0, 0 : 4 * STRIPE], ws.at[2])
     sent(wall.at[:, 0], ws.at[3])
     for k in range(len(SPLITS)):
-        for p in range(2):
-            sent(bufs[k].at[p, 0:3], p1s.at[k * 2 + p])
-            sent(twos[k].at[p, 0:3], p2s.at[k * 2 + p])
-            sent(outs3[k].at[p], p3s.at[k * 2 + p])
-    for group in range(2):
-        for p in range(2):
-            sent(amount(p, group, 96), a1s.at[group * 2 + p])
-            sent(amount(p, group, 256), a2s.at[group * 2 + p])
-            sent(amount(p, group, 128), a3s.at[group * 2 + p])
+        sent(bufs[k].at[:, 0:3], p1s.at[k])
+        sent(twos[k].at[:, 0:3], p2s.at[k])
+        sent(outs3[k], p3s.at[k])
+    for sem, rows in ((a1s, 96), (a2s, 256), (a3s, 128)):
+        sent(ag.at[:, 0:rows], sem.at[0])
     for stage in range(3):
-        sent(taps.at[stage, 0:3], tss.at[stage])
+        sent(taps.at[stage, 0:3, 0:6], tss.at[stage])
     sent(tfin.at[0], tss.at[3])
     sent(gsend.at[0], gss.at[0])
     combine(7, *units[7])
@@ -550,26 +552,27 @@
         copies.append(copy)
         return copy
 
-    tap_load = start(tap_in, tap)
+    gi_load = start(gi_in, gi)
     loads = []
     for i in range(count):
         part = pl.ds(i * rows, rows)
         loads.append(start(ag_in.at[:, part], half.at[:, part]))
-    gi_load = start(gi_in, gi)
-    tap_load.wait()
-    for side in range(2):
-        cols = slice(side * COLS, side * COLS + COLS)
-        tg[:, cols] = tap[side, 0:3]
-        tu[:, cols] = tap[side, 3:6]
-    stores = [start(tg, tap_gate), start(tu, tap_up)]
+    tap_load = start(tap_in, tap)
+    gi_load.wait()
+    stores = [start(gi, gi_out.at[0])]
     for i in range(count):
         part = pl.ds(i * rows, rows)
         loads[i].wait()
         for p, target in enumerate((gate_out, up_out)):
             full[p, part] = half[p, part].astype(f32) * (float(TOKENS) ** -0.5)
             stores.append(start(full.at[p, part], target.at[part]))
-    gi_load.wait()
-    stores.append(start(gi, gi_out.at[0]))
+        if i == count // 2:
+            tap_load.wait()
+            for side in range(2):
+                cols = slice(side * COLS, side * COLS + COLS)
+                tg[:, cols] = tap[side, 0:3]
+                tu[:, cols] = tap[side, 3:6]
+            stores += [start(tg, tap_gate), start(tu, tap_up)]
     for copy in stores:
         copy.wait()
 
@@ -591,9 +594,9 @@
         + [pltpu.VMEM((2, 8, HALF, 256), bf16), pltpu.VMEM((8, HALF, 256), bf16), pltpu.VMEM((8, HALF, 256), bf16)]
         + [pltpu.VMEM((3, 2 * COLS), bf16)] * 2
         + [dma((14,)), dma((3,)), dma((2,)), dma((4,)), dma((2,)), dma((4,)), dma((2 * len(FAR),)), dma((4,)), dma((4,))]
-        + [dma((2 * count,)), dma((6 * count,))] * 2
-        + [dma((2 * count,)), dma((2 * count,))]
-        + [dma((4,)), dma((12,)), dma((4,)), dma((16,)), dma((4,)), dma((4,)), dma((4,)), dma((4,)), dma((1,)), dma((8,))]
+        + [dma((count,)), dma((6 * count,))] * 2
+        + [dma((count,)), dma((count,))]
+        + [dma((1,)), dma((9,)), dma((1,)), dma((12,)), dma((1,)), dma((3,)), dma((4,)), dma((4,)), dma((1,)), dma((8,))]
     )
     grad_inputs, sums, tap_sums = pl.pallas_call(
         kernel,

time: 112 us -> 111 us (level)
  no operation moved by 1% of the time
where the time goes in v4:
time: 111 us
  Pallas kernels  111 us (100%)
    pallas_call x1, Pallas kernels, per_device(): pl.pallas_call(kernel, out_shape=(jax.ShapeDtypeStruct((HALF, WIDTH), bf1...  106 us
    pallas_call x1, Pallas kernels, per_device(): pl.pallas_call(finish, out_shape=(jax.ShapeDtypeStruct((1, HALF, WIDTH),...  4.68 us

profile of v4, /device:TPU:1, one launch (start us, length us, event | category | flops | bytes accessed | tf_op | source)
XLA Modules:
  0.0 111.4 jit_solution(14541021467741990889)
XLA Ops:
  0.6 105.9 %shard_map.119 = (bf16[384,2048]{1,0:T(8,128)(2,1)}, bf16[2,512,1408]{2,1,0:T(8,128)(2,1)}, f32[2,8,1408]{2,1,0:T(8,128)}) custom-call(bf16[1,384,2048]{2,1,0:T(8,128)(2,1)} %x_hbm.1, bf16[1,768,1408]{2,1,0:T(8,128)(2,1)} %pg_hbm.1, bf16[1,768,1408]{2,1,0:T(8,128)(2,1)} %pu_hbm.1, bf16[1,768,1408]{2,1,0:T(8,128)(2,1)} %ct_hbm.1, bf16[512,1408]{1,0:T(8,128)(2,1)} %wg_hbm.1, ...), custom_call_target="tpu_custom_call" | custom-call | tf_op jit(solution)/shard_map/pallas_call | solution.py:601
  106.5 4.7 %shard_map.120 = (bf16[1,384,2048]{2,1,0:T(8,128)(2,1)}, f32[512,1408]{1,0:T(8,128)}, f32[512,1408]{1,0:T(8,128)}, f32[3,2816]{1,0:T(4,128)}, f32[3,2816]{1,0:T(4,128)}) custom-call(bf16[384,2048]{1,0:T(8,128)(2,1)} %get-tuple-element.8.gi_in, bf16[2,512,1408]{2,1,0:T(8,128)(2,1)} %get-tuple-element.9.ag_in, f32[2,8,1408]{2,1,0:T(8,128)} %get-tuple-element.10.tap_in), custom_call_target="tpu_custom_call" | custom-call | tf_op jit(solution)/shard_map/pallas_call | solution.py:616

commit v5 on v4

--- a/solution.py
+++ b/solution.py
@@ -12,7 +12,7 @@
 COLS = 1408
 WIDTH = 2048
 TOKENS = 49152
-SPLITS = ((0, 256), (256, 512), (768, 640))
+SPLITS = ((0, 384), (384, 512), (896, 512))
 CHUNK = 64
 PAD = 16
 STRIPE = 32
@@ -428,7 +428,7 @@
 
     for copy in tap_loads + pre[0]:
         copy.wait()
-    elementwise(0, 0, 2)
+    elementwise(0, 0, 3)
     x_local.wait()
     turn_half(c, 8, early)
     other_half = xs.at[pl.ds(mult(wrap(c + 1, 2) * HALF, HALF), HALF)]
@@ -439,9 +439,9 @@
     step0(0)
     for copy in pre[1]:
         copy.wait()
-    elementwise(1, 0, 2)
+    elementwise(1, 0, 1)
     stripe_start()
-    elementwise(1, 2, 4)
+    elementwise(1, 1, 4)
     step0(1)
     turn_half(0, 12, late)
     turn_half(1, 12, late)
@@ -450,7 +450,7 @@
         copy.wait()
     elementwise(2, 0, 2)
     stripe_pass()
-    elementwise(2, 2, 5)
+    elementwise(2, 2, 4)
     step0(2)
     step1(1, 1)
     step1(0, 2)

time: 111 us -> 111 us (level)
  no operation moved by 1% of the time
where the time goes in v5:
time: 111 us
  Pallas kernels  110 us (99%)
    pallas_call x1, Pallas kernels, per_device(): pl.pallas_call(kernel, out_shape=(jax.ShapeDtypeStruct((HALF, WIDTH), bf1...  105 us
    pallas_call x1, Pallas kernels, per_device(): pl.pallas_call(finish, out_shape=(jax.ShapeDtypeStruct((1, HALF, WIDTH),...  4.68 us

profile of v5, /device:TPU:1, one launch (start us, length us, event | category | flops | bytes accessed | tf_op | source)
XLA Modules:
  0.0 110.7 jit_solution(13452369725355798735)
XLA Ops:
  0.6 105.3 %shard_map.119 = (bf16[384,2048]{1,0:T(8,128)(2,1)}, bf16[2,512,1408]{2,1,0:T(8,128)(2,1)}, f32[2,8,1408]{2,1,0:T(8,128)}) custom-call(bf16[1,384,2048]{2,1,0:T(8,128)(2,1)} %x_hbm.1, bf16[1,768,1408]{2,1,0:T(8,128)(2,1)} %pg_hbm.1, bf16[1,768,1408]{2,1,0:T(8,128)(2,1)} %pu_hbm.1, bf16[1,768,1408]{2,1,0:T(8,128)(2,1)} %ct_hbm.1, bf16[512,1408]{1,0:T(8,128)(2,1)} %wg_hbm.1, ...), custom_call_target="tpu_custom_call" | custom-call | tf_op jit(solution)/shard_map/pallas_call | solution.py:601
  105.9 4.7 %shard_map.120 = (bf16[1,384,2048]{2,1,0:T(8,128)(2,1)}, f32[512,1408]{1,0:T(8,128)}, f32[512,1408]{1,0:T(8,128)}, f32[3,2816]{1,0:T(4,128)}, f32[3,2816]{1,0:T(4,128)}) custom-call(bf16[384,2048]{1,0:T(8,128)(2,1)} %get-tuple-element.8.gi_in, bf16[2,512,1408]{2,1,0:T(8,128)(2,1)} %get-tuple-element.9.ag_in, f32[2,8,1408]{2,1,0:T(8,128)} %get-tuple-element.10.tap_in), custom_call_target="tpu_custom_call" | custom-call | tf_op jit(solution)/shard_map/pallas_call | solution.py:616
